TPU v7x, 32 devices: a whole 2x2x4 slice. The times are simulated.
32 devices in a mesh: sp: 8 (over z, y), tp: 4 (over x, core).
Axes of the slice: x: 2, y: 2, z: 4, core: 2. Of those that a mesh axis runs over, the one named last changes fastest.
Arguments:
- stream: bfloat16 [4096, 2048], P(('sp', 'tp')), may hold values from -6 to 6
- conv_value: bfloat16 [4096, 512], P('sp', 'tp'), may hold values from -6 to 6
- conv_gate: bfloat16 [4096, 512], P('sp', 'tp'), may hold values from -8 to 8
- doc_ids: int32 [4096], P('sp'), may hold values from 0 to 3, never falling along the last dimension, each value on 1 to 2048 neighbouring positions
- conv_taps: float32 [31, 512], P(None, 'tp'), may hold values from -2.2 to 2.2
- conv_bias: float32 [512], P('tp'), may hold values from -3 to 3
- chan_gain: float32 [512], replicated, may hold values from 0.1 to 1.9
- chan_shift: float32 [512], replicated, may hold values from -3 to 3
- out_weight: bfloat16 [512, 2048], replicated, may hold values from -0.25 to 0.25
- rms_gain: float32 [2048], replicated, may hold values from 0.1 to 1.9
- expert_ids: int32 [4096, 2], P(('sp', 'tp')), may hold values from 0 to 15, all different within a row; in each aligned block of 128 rows (0 to 127, 128 to 255, ...) at most 24 rows name the same one
- group_prob: float32 [4096], P(('sp', 'tp')), may hold values from 0.3 to 1
- route_logits: float32 [4096, 2], P(('sp', 'tp')), may hold values from -6 to 6
- expert_gate: bfloat16 [16, 2048, 1024], P('sp', None, 'tp'), may hold values from -0.125 to 0.125
- expert_up: bfloat16 [16, 2048, 1024], P('sp', None, 'tp'), may hold values from -0.125 to 0.125
- expert_down: bfloat16 [16, 1024, 2048], P('sp', 'tp'), may hold values from -0.1875 to 0.1875
Outputs:
- mixed: bfloat16 [4096, 2048], P(('sp', 'tp'))
Inputs may be any that keep to these rules, and one draw needn't show every extreme that they name: `expert_ids`: each row names 2 different experts. In each aligned block of 128 rows (the rows of one device) no expert is named by more than 24 rows, a bound that some block reaches. `doc_ids`: document numbers never fall along the sequence; every document has 1 to 2048 positions, one exactly 2048.
All inputs are finite; a program needn't handle non-finite values.
Results may differ from a plain program's by a relative error of at most 0.012.
Values may be sent and summed in bfloat16 or wider, within the bound.
A program may use at most 64 MiB of HBM per device.

v0:
```python
import jax
import jax.numpy as jnp
from jax import lax
from jax.sharding import PartitionSpec as P

CONV_CH = 512


eps = 1e-06


def passed_along(x, axis, by):
    size = lax.axis_size(axis)
    pairs = [(i, i + by) for i in range(size) if 0 <= i + by < size]
    return lax.ppermute(x, axis, pairs)


def causal_conv(values, gates, docs, conv_taps, conv_bias):
    reach = conv_taps.shape[0] - 1
    acts = values.astype(jnp.float32) * jax.nn.sigmoid(gates.astype(jnp.float32))
    total = values.shape[0] - reach
    result = jnp.broadcast_to(conv_bias[None, :], (total, values.shape[1]))
    own_doc = docs[reach:]
    for offset in range(reach + 1):
        begin = reach - offset
        same = (docs[begin : begin + total] == own_doc)[:, None]
        result = (
            result + jnp.where(same, acts[begin : begin + total], 0.0) * conv_taps[offset][None, :]
        )
    return result.astype(jnp.bfloat16)


def finish_norm(values, mean, square, gain, shift):
    spread = square - mean * mean
    scaled = (values - mean) * lax.rsqrt(spread + eps) * gain + shift
    return jax.nn.silu(scaled).astype(jnp.bfloat16)


def apply_experts(arrived, expert_gate, expert_up, expert_down):
    outputs = []
    for local in range(arrived.shape[1]):
        rows = arrived[:, local].reshape(-1, arrived.shape[3])
        gated = jnp.dot(rows, expert_gate[local], preferred_element_type=jnp.float32)
        upward = jnp.dot(rows, expert_up[local], preferred_element_type=jnp.float32)
        hidden = (jax.nn.silu(gated) * upward).astype(jnp.bfloat16)
        partial_value = jnp.dot(hidden, expert_down[local], preferred_element_type=jnp.float32)
        outputs.append(partial_value.reshape(arrived.shape[0], arrived.shape[2], arrived.shape[3]))
    return jnp.stack(outputs, axis=1)


def split_quarters(partial_value, quarters):
    shape = partial_value.shape
    return partial_value.astype(jnp.bfloat16).reshape(
        shape[0], shape[1], quarters, shape[2] // quarters, shape[3]
    )


def body(
    stream,
    conv_value,
    conv_gate,
    doc_ids,
    conv_taps,
    conv_bias,
    chan_gain,
    chan_shift,
    out_weight,
    rms_gain,
    expert_ids,
    group_prob,
    route_logits,
    expert_gate,
    expert_up,
    expert_down,
):
    reach = conv_taps.shape[0] - 1
    tail_value, tail_gate, tail_doc = passed_along(
        (conv_value[-reach:], conv_gate[-reach:], doc_ids[-reach:]), "sp", 1
    )
    values = jnp.concatenate([tail_value, conv_value], axis=0)
    gates = jnp.concatenate([tail_gate, conv_gate], axis=0)
    docs = jnp.concatenate([tail_doc, doc_ids], axis=0)
    conved = causal_conv(values, gates, docs, conv_taps, conv_bias)
    own_rows = stream.shape[0]
    width_local = conved.shape[1]
    lane = lax.axis_index("tp") * width_local
    floats = conved.astype(jnp.float32)
    sums, squares = lax.psum((jnp.sum(floats, axis=1), jnp.sum(floats * floats, axis=1)), "tp")
    mean = (sums / CONV_CH)[:, None]
    square = (squares / CONV_CH)[:, None]
    gain = lax.dynamic_slice_in_dim(chan_gain, lane, width_local, 0)
    shift = lax.dynamic_slice_in_dim(chan_shift, lane, width_local, 0)
    activated = finish_norm(floats, mean, square, gain, shift)
    weight_rows = lax.dynamic_slice_in_dim(out_weight, lane, width_local, 0)
    projected = lax.psum_scatter(
        jnp.dot(activated, weight_rows, preferred_element_type=jnp.float32).astype(jnp.bfloat16),
        "tp",
        scatter_dimension=0,
        tiled=True,
    ).astype(jnp.float32)
    resid = (stream.astype(jnp.float32) + projected).astype(jnp.bfloat16)
    resid_float = resid.astype(jnp.float32)
    mean_square = jnp.mean(resid_float * resid_float, axis=-1, keepdims=True)
    normed = (resid_float * lax.rsqrt(mean_square + eps) * rms_gain).astype(jnp.bfloat16)
    gap = route_logits[:, 0] - route_logits[:, 1]
    weights = jnp.stack(
        [group_prob * jax.nn.sigmoid(gap), group_prob * jax.nn.sigmoid(-gap)], axis=1
    )
    sp_count = lax.axis_size("sp")
    tp_count = lax.axis_size("tp")
    local_experts = expert_gate.shape[0]
    experts_all = sp_count * local_experts
    top_count = expert_ids.shape[1]
    capacity = max(2, 3 * own_rows * top_count // (2 * experts_all))
    flat_ids = expert_ids.reshape(-1)
    onehot = (flat_ids[:, None] == jnp.arange(experts_all, dtype=jnp.int32)[None, :]).astype(
        jnp.int32
    )
    earlier = jnp.cumsum(onehot, axis=0) - onehot
    ranks = jnp.sum(earlier * onehot, axis=1)
    dest = flat_ids * capacity + ranks
    route_token = jnp.arange(flat_ids.shape[0], dtype=jnp.int32) // top_count
    source = jnp.full((experts_all * capacity,), own_rows, jnp.int32).at[dest].set(route_token)
    with_blank = jnp.concatenate([normed, jnp.zeros((1, normed.shape[1]), jnp.bfloat16)], axis=0)
    outgoing = with_blank[source].reshape(sp_count, local_experts, capacity, normed.shape[1])
    arrived_own = lax.all_to_all(outgoing, "sp", split_axis=0, concat_axis=0, tiled=True)
    arrived = lax.all_gather(arrived_own, "tp", axis=2, tiled=True)
    partial_value = apply_experts(arrived, expert_gate, expert_up, expert_down)
    quarters = lax.all_to_all(
        split_quarters(partial_value, tp_count), "tp", split_axis=2, concat_axis=2, tiled=True
    )
    summed = jnp.sum(quarters.astype(jnp.float32), axis=2).astype(jnp.bfloat16)
    routed = lax.all_to_all(summed, "sp", split_axis=0, concat_axis=0, tiled=True)
    flat_out = routed.reshape(experts_all * capacity, normed.shape[1])
    picked = flat_out[dest].reshape(own_rows, top_count, normed.shape[1]).astype(jnp.float32)
    combined = jnp.sum(weights[:, :, None] * picked, axis=1)
    return (resid_float + combined).astype(jnp.bfloat16)


def solution(mesh):
    placed = (
        P(("sp", "tp"), None),
        P("sp", "tp"),
        P("sp", "tp"),
        P("sp"),
        P(None, "tp"),
        P("tp"),
        P(),
        P(),
        P(),
        P(),
        P(("sp", "tp"), None),
        P(("sp", "tp")),
        P(("sp", "tp"), None),
        P("sp", None, "tp"),
        P("sp", None, "tp"),
        P("sp", "tp", None),
    )
    return jax.shard_map(
        body, mesh=mesh, in_specs=placed, out_specs=P(("sp", "tp"), None), check_vma=False
    )
```

profile of v0, /device:TPU:0, one launch (start us, length us, event | category | flops | bytes accessed | tf_op | source)
XLA Modules:
  0.0 321.5 jit_solution(74922192068838987)
XLA Ops:
  6.5 0.0 reduce-scatter.2.cloned.1.call-start
  6.5 0.9 slice.325
  7.4 4.9 %collective-permute-start.2 = (s32[30]{0:T(128)S(1)}, s32[30]{0:T(128)S(1)}, u32[]{:S(2)}, u32[]{:S(2)}) collective-permute-start(s32[30]{0:T(128)S(1)} %slice.325), channel_id=1, source_target_pairs={{0,4},{4,8},{8,12},{12,16},{16,20},{20,24},{24,28},{1,5},{5,9},{9,... | collective-permute-start | bytes 368 | tf_op jit(solution)/shard_map/ppermute | solution.py:15
  12.3 0.7 slice.321
  13.0 3.4 %collective-permute-start = (bf16[30,128]{1,0:T(8,128)(2,1)S(1)}, bf16[30,128]{1,0:T(8,128)(2,1)S(1)}, u32[]{:S(2)}, u32[]{:S(2)}) collective-permute-start(bf16[30,128]{1,0:T(8,128)(2,1)S(1)} %slice.321), channel_id=1, source_target_pairs={{0,4},{4,8},{8,12},{12,16},{16,20},{20,24},{24,28},{1,5},{5,9},{9,... | collective-permute-start | bytes 23048 | tf_op jit(solution)/shard_map/ppermute | solution.py:15
  16.5 0.7 slice.322
  17.2 3.4 %collective-permute-start.1 = (bf16[30,128]{1,0:T(8,128)(2,1)S(1)}, bf16[30,128]{1,0:T(8,128)(2,1)S(1)}, u32[]{:S(2)}, u32[]{:S(2)}) collective-permute-start(bf16[30,128]{1,0:T(8,128)(2,1)S(1)} %slice.322), channel_id=1, source_target_pairs={{0,4},{4,8},{8,12},{12,16},{16,20},{20,24},{24,28},{1,5},{5,9},{9,... | collective-permute-start | bytes 23048 | tf_op jit(solution)/shard_map/ppermute | solution.py:15
  20.6 1.0 slice_bitcast_fusion.30
  21.6 1.0 slice_bitcast_fusion.29
  22.6 0.8 dynamic_slice.10
  23.3 0.8 dynamic_slice.9
  24.1 0.0 collective-permute-done.2
  24.1 0.8 pad_add_fusion
  24.8 0.8 slice_compare_fusion.29
  25.6 0.8 slice_compare_fusion.28
  26.4 0.0 collective-permute-done
  26.4 0.0 collective-permute-done.1
  26.4 1.1 divide_multiply_fusion
  27.5 3.8 %convert_reduce_fusion = (f32[512]{0:T(512)S(1)}, f32[512]{0:T(512)S(1)}, bf16[512,128]{1,0:T(8,128)(2,1)S(1)}) fusion(f32[128]{0:T(128)S(1)} %get-tuple-element.41, f32[542,128]{1,0:T(8,128)S(1)} %divide_multiply_fusion, pred[512]{0:T(512)(128)(4,1)S(1)} %get-tuple-element.71, f32[128]{0:T(128)S(1)} %get-tuple-element.42, ...), kind=kLoop, calls=%fused_computation.39 | loop fusion | flops 6355968 | bytes 8293376 | tf_op jit(solution)/shard_map/reduce_sum | solution.py:88
  31.3 0.0 copy-start.4
  31.4 0.0 copy-start.1
  31.4 5.9 %all-reduce.1 = (f32[512]{0:T(512)S(1)}, f32[512]{0:T(512)S(1)}) all-reduce(f32[512]{0:T(512)S(1)} %get-tuple-element.6, f32[512]{0:T(512)S(1)} %get-tuple-element.5), channel_id=1, replica_groups=mesh['sp'=8,'tp'=4] {'tp'}, use_global_device_ids=true, to_apply=%region_3.4 | all-reduce | flops 1024 | bytes 8192 | tf_op jit(solution)/shard_map/psum | solution.py:88
  37.3 2.1 convolution_convert_fusion.2
  39.4 0.0 reduce-scatter.2.cloned.1.call-update
  39.4 0.0 all-gather.2.cloned.1.call-start
  39.5 0.1 copy.33
  39.6 0.1 eq.149
  39.8 0.1 eq.145
  39.9 0.6 reduce-window.6
  40.5 0.2 slice_reduce_fusion
  40.7 0.1 copy.32
  40.8 0.1 mul.520
  41.0 0.1 fusion.103
  41.1 1.4 scatter_custom_fusion
  42.5 27.7 %reduce-scatter.2.cloned.1.call-done = bf16[128,2048]{1,0:T(8,128)(2,1)} async-done(((bf16[512,2048]{1,0:T(8,128)(2,1)}), bf16[128,2048]{1,0:T(8,128)(2,1)}) %reduce-scatter.2.cloned.1.call-update) | async-done | bytes 524304 | tf_op jit(solution)/shard_map/reduce_scatter | solution.py:95
  70.2 1.3 fusion.4
  71.5 1.3 fusion.6
  72.8 3.1 gather_fusion
  76.0 42.4 %all_to_all.15 = bf16[8,2,24,2048]{3,2,1,0:T(8,128)(2,1)} all-to-all(bf16[8,2,24,2048]{3,2,1,0:T(8,128)(2,1)} %bitcast.137), channel_id=1, replica_groups=mesh['sp'=8,'tp'=4] {'sp'}, dimensions={0} | all-to-all | bytes 3145728 | tf_op jit(solution)/shard_map/all_to_all | solution.py:126
  118.4 0.0 all-gather.2.cloned.1.call-update
  118.4 44.6 %all-gather.2.cloned.1.call-done = bf16[8,2,96,2048]{3,2,1,0:T(8,128)(2,1)} async-done(((bf16[8,2,24,2048]{3,2,1,0:T(8,128)(2,1)}), bf16[8,2,96,2048]{3,2,1,0:T(8,128)(2,1)}) %all-gather.2.cloned.1.call-update) | async-done | bytes 6291472 | tf_op jit(solution)/shard_map/all_gather | solution.py:127
  163.0 3.6 %fusion.112 = (bf16[8,1,96,2048]{3,2,1,0:T(8,128)(2,1)S(1)}, bf16[8,1,96,2048]{3,2,1,0:T(8,128)(2,1)S(1)}) fusion(bf16[8,2,96,2048]{3,2,1,0:T(8,128)(2,1)} %all-gather.2.cloned.1.call-done), kind=kLoop, calls=%fused_computation.242 | loop fusion | bytes 12582912 | tf_op jit(solution)/shard_map/slice | solution.py:42
  166.6 1.0 fusion.14
  167.6 0.0 copy-start.8
  167.6 1.0 fusion.11
  168.6 0.6 copy-done.8
  169.2 1.0 fusion.2
  170.2 0.0 copy-start.9
  170.2 1.0 fusion.3
  171.2 0.6 copy-done.9
  171.8 1.0 fusion
  172.8 1.0 fusion.1
  173.8 0.6 pad_maximum_fusion
  174.4 1.1 copy.36
  175.5 74.2 %all_to_all.16 = bf16[8,2,4,24,2048]{4,3,0,1,2:T(8,128)(2,1)} all-to-all(bf16[8,2,4,24,2048]{4,3,0,1,2:T(8,128)(2,1)S(1)} %copy.36), channel_id=1, replica_groups=mesh['sp'=8,'tp'=4] {'tp'}, dimensions={2} | all-to-all | bytes 12582912 | tf_op jit(solution)/shard_map/all_to_all | solution.py:129
  249.7 5.7 %reduce_sum.64 = bf16[8,2,24,2048]{3,2,0,1:T(8,128)(2,1)} reduce(bf16[8,2,4,24,2048]{4,3,0,1,2:T(8,128)(2,1)} %all_to_all.16, bf16[]{:T(256)} %constant.56.clone.1), dimensions={2}, to_apply=%region_10.11 | reduce | flops 2359296 | bytes 7864322 | tf_op jit(solution)/shard_map/reduce_sum | solution.py:132
  255.4 2.8 copy.38
  258.1 5.5 %all-to-all-start.2 = ((bf16[8,2,24,2048]{3,2,1,0:T(8,128)(2,1)}), bf16[8,2,24,2048]{3,2,1,0:T(8,128)(2,1)}, u32[]{:S(2)}, u32[]{:S(2)}) async-start(bf16[8,2,24,2048]{3,2,1,0:T(8,128)(2,1)} %copy.38), calls=%async_computation.3 | async-start | bytes 3145728 | tf_op jit(solution)/shard_map/all_to_all | solution.py:133
  263.7 0.1 copy.31
  263.8 36.6 %all-to-all-done.2 = bf16[8,2,24,2048]{3,2,1,0:T(8,128)(2,1)} async-done(((bf16[8,2,24,2048]{3,2,1,0:T(8,128)(2,1)}), bf16[8,2,24,2048]{3,2,1,0:T(8,128)(2,1)}, u32[]{:S(2)}, u32[]{:S(2)}) %all-to-all-start.2) | async-done | bytes 1572896 | tf_op jit(solution)/shard_map/all_to_all | solution.py:133
  300.4 5.0 %gather_fusion.1 = bf16[256,2048]{1,0:T(8,128)(2,1)} fusion(bf16[384,2048]{1,0:T(8,128)(2,1)} %bitcast.55, s32[1024]{0:T(1024)S(1)} %pad_clamp_fusion), kind=kCustom, calls=%fused_computation.1 | custom fusion | bytes 2098176 | tf_op jit(solution)/shard_map/gather | solution.py:135
  305.4 3.5 %reshape.150 = f32[128,2,2048]{2,1,0:T(2,128)} reshape(bf16[256,2048]{1,0:T(8,128)(2,1)} %gather_fusion.1) | data formatting | bytes 3145728 | tf_op jit(solution)/shard_map/convert_element_type | solution.py:135
  308.8 4.8 %multiply_reduce_fusion = f32[128,2048]{1,0:T(8,128)S(1)} fusion(f32[128,2,2048]{2,1,0:T(2,128)} %reshape.150, f32[128,2]{1,0:T(8,128)S(1)} %copy.31), kind=kLoop, calls=%fused_computation.9 | loop fusion | flops 786432 | bytes 3146752 | tf_op jit(solution)/shard_map/reduce_sum | solution.py:136
  313.6 1.0 fusion.7
  (28 shorter events, 0.2 us)
Async XLA Ops:
  6.5 30.7 %copy-start = (bf16[512,2048]{1,0:T(8,128)(2,1)S(1)}, bf16[512,2048]{1,0:T(8,128)(2,1)}, u32[]{:S(2)}) copy-start(bf16[512,2048]{1,0:T(8,128)(2,1)} %param.24) | copy-start | bytes 6291460
  6.5 63.7 %reduce-scatter.2.cloned.1.call-start = ((), (), s32[]{:S(2)}) async-start(), calls=%async_computation.4 | async-start | bytes 2621440 | tf_op jit(solution)/shard_map/reduce_scatter | solution.py:95
  7.4 16.6 %collective-permute-start.2 = (s32[30]{0:T(128)S(1)}, s32[30]{0:T(128)S(1)}, u32[]{:S(2)}, u32[]{:S(2)}) collective-permute-start(s32[30]{0:T(128)S(1)} %slice.325), channel_id=1, source_target_pairs={{0,4},{4,8},{8,12},{12,16},{16,20},{20,24},{24,28},{1,5},{5,9},{9,... | collective-permute-start | bytes 368 | tf_op jit(solution)/shard_map/ppermute | solution.py:15
  13.0 13.4 %collective-permute-start = (bf16[30,128]{1,0:T(8,128)(2,1)S(1)}, bf16[30,128]{1,0:T(8,128)(2,1)S(1)}, u32[]{:S(2)}, u32[]{:S(2)}) collective-permute-start(bf16[30,128]{1,0:T(8,128)(2,1)S(1)} %slice.321), channel_id=1, source_target_pairs={{0,4},{4,8},{8,12},{12,16},{16,20},{20,24},{24,28},{1,5},{5,9},{9,... | collective-permute-start | bytes 23048 | tf_op jit(solution)/shard_map/ppermute | solution.py:15
  17.2 9.2 %collective-permute-start.1 = (bf16[30,128]{1,0:T(8,128)(2,1)S(1)}, bf16[30,128]{1,0:T(8,128)(2,1)S(1)}, u32[]{:S(2)}, u32[]{:S(2)}) collective-permute-start(bf16[30,128]{1,0:T(8,128)(2,1)S(1)} %slice.322), channel_id=1, source_target_pairs={{0,4},{4,8},{8,12},{12,16},{16,20},{20,24},{24,28},{1,5},{5,9},{9,... | collective-permute-start | bytes 23048 | tf_op jit(solution)/shard_map/ppermute | solution.py:15
  31.3 8.1 %copy-start.4 = (s32[128,2]{0,1:T(2,128)S(1)}, s32[128,2]{0,1:T(2,128)}, u32[]{:S(2)}) copy-start(s32[128,2]{0,1:T(2,128)} %param.26) | copy-start | bytes 3076
  31.4 38.9 %copy-start.1 = (bf16[128,2048]{1,0:T(8,128)(2,1)S(1)}, bf16[128,2048]{1,0:T(8,128)(2,1)}, u32[]{:S(2)}) copy-start(bf16[128,2048]{1,0:T(8,128)(2,1)} %param.16) | copy-start | bytes 1572868
  37.3 34.3 %copy-start.3 = (f32[2048]{0:T(1024)S(1)}, f32[2048]{0:T(1024)}, u32[]{:S(2)}) copy-start(f32[2048]{0:T(1024)} %param.25) | copy-start | bytes 24580
  39.4 123.6 %all-gather.2.cloned.1.call-start = ((), (), s32[]{:S(2)}) async-start(), calls=%async_computation.5 | async-start | bytes 7864320 | tf_op jit(solution)/shard_map/all_gather | solution.py:127
  163.0 3.6 %copy-start.7 = (bf16[2,2048,256]{2,1,0:T(8,128)(2,1)S(1)}, bf16[2,2048,256]{2,1,0:T(8,128)(2,1)}, u32[]{:S(2)}) copy-start(bf16[2,2048,256]{2,1,0:T(8,128)(2,1)} %param.29) | copy-start | bytes 6291460
  167.6 1.6 copy-start.8
  170.2 1.6 copy-start.9
  255.4 8.3 %copy-start.5 = (f32[128,2]{0,1:T(2,128)S(1)}, f32[128,2]{0,1:T(2,128)}, u32[]{:S(2)}) copy-start(f32[128,2]{0,1:T(2,128)} %param.28) | copy-start | bytes 3076
  255.4 8.3 %copy-start.6 = (f32[128]{0:T(128)S(1)}, f32[128]{0:T(128)}, u32[]{:S(2)}) copy-start(f32[128]{0:T(128)} %param.27) | copy-start | bytes 1540
  258.1 42.3 %all-to-all-start.2 = ((bf16[8,2,24,2048]{3,2,1,0:T(8,128)(2,1)}), bf16[8,2,24,2048]{3,2,1,0:T(8,128)(2,1)}, u32[]{:S(2)}, u32[]{:S(2)}) async-start(bf16[8,2,24,2048]{3,2,1,0:T(8,128)(2,1)} %copy.38), calls=%async_computation.3 | async-start | bytes 3145728 | tf_op jit(solution)/shard_map/all_to_all | solution.py:133
  305.4 8.3 %copy-start.2 = (bf16[128,2048]{1,0:T(8,128)(2,1)S(1)}, bf16[128,2048]{1,0:T(8,128)(2,1)}, u32[]{:S(2)}) copy-start(bf16[128,2048]{1,0:T(8,128)(2,1)} %reduce-scatter.2.cloned.1.call-done) | copy-start | bytes 1572868
Sparse Core Ops, SparseCore 0:
  39.6 30.6 reduce-scatter.1
  118.6 44.4 all-gather.1
where the time goes:
time: 322 us; the launch traced here: 321 us
  blocking collectives  123 us (38%)
  waiting for transfers between devices  109 us (34%)
  local copies, waits for them, and re-layouts  28.4 us (9%)
  other arithmetic  22.6 us (7%)
  starting transfers between devices  17.3 us (5%)
  between operations  13.7 us (4%)
  matrix products  8.06 us (3%)
    all_to_all x1, blocking collectives, body(): lax.all_to_all(split_quarters(partial_value, tp_count), 'tp', split_axis=...  74.2 us
    all_gather x1, waiting for transfers between devices, body(): arrived = lax.all_gather(arrived_own, 'tp', axis=2, tiled=True)  44.6 us
    all_to_all x1, blocking collectives, body(): lax.all_to_all(outgoing, 'sp', split_axis=0, concat_axis=0, tiled=True)  42.4 us
    all_to_all x1, waiting for transfers between devices, body(): lax.all_to_all(summed, 'sp', split_axis=0, concat_axis=0, tiled=True)  36.6 us
    reduce_scatter x1, waiting for transfers between devices, body(): lax.psum_scatter(jnp.dot(activated, weight_rows, preferred_element_type=j...  27.7 us
    ppermute x3, starting transfers between devices, passed_along(): return lax.ppermute(x, axis, pairs)  11.7 us
  transfers between devices with their start and end apart: 6, of which 3 were waited for; matrix products, arithmetic and copies ran while one was open for 3% of the time, Pallas kernels for 0%

commit v1 on v0

v1 whole, which is shorter than its diff:
```python
import jax
import jax.numpy as jnp
from jax import lax
from jax.sharding import Mesh, PartitionSpec as P

eps = 1e-06
F32, BF16 = jnp.float32, jnp.bfloat16


def swap(x, axis, by):
    size = lax.axis_size(axis)
    return lax.ppermute(x, axis, [(i, (i + by) % size) for i in range(size)])


def gather_pieces(weight):
    nx, nc = lax.axis_size("tx"), lax.axis_size("tc")
    me = lax.axis_index("tx")
    pieces = []
    for by in range(nx):
        piece = lax.dynamic_index_in_dim(weight, lax.rem(me + by, nx), 0, keepdims=False)
        pieces.append(piece if by == 0 else swap(piece, "tx", by))
    return pieces + [swap(p, "tc", by) for by in range(1, nc) for p in pieces]


def body(
    stream, conv_value, conv_gate, doc_ids, conv_taps, conv_bias, chan_gain, chan_shift, out_weight,
    rms_gain, expert_ids, group_prob, route_logits, expert_gate, expert_up, expert_down,
):
    reach = conv_taps.shape[0] - 1
    tp = ("tx", "tc")
    own_rows, width = stream.shape
    sp_count = lax.axis_size("sp")
    block, chans = conv_value.shape
    docs_row = doc_ids.astype(BF16)
    tail = jnp.concatenate(
        [conv_value[-reach:], conv_gate[-reach:], jnp.broadcast_to(docs_row[-reach:, None], (reach, chans))], axis=0
    )
    tail = lax.ppermute(tail, "sp", [(i, i + 1) for i in range(sp_count - 1)])
    gates_w, ups_w, downs_w = gather_pieces(expert_gate), gather_pieces(expert_up), gather_pieces(expert_down)

    values = jnp.concatenate([tail[:reach], conv_value], axis=0).astype(F32)
    gates = jnp.concatenate([tail[reach : 2 * reach], conv_gate], axis=0).astype(F32)
    docs = jnp.concatenate([tail[2 * reach :, 0], docs_row], axis=0)
    acts = values * jax.nn.sigmoid(gates)
    result = jnp.broadcast_to(conv_bias[None, :], (block, chans))
    for offset in range(reach + 1):
        begin = reach - offset
        same = (docs[begin : begin + block] == docs_row)[:, None]
        result = result + jnp.where(same, acts[begin : begin + block], 0.0) * conv_taps[offset][None, :]
    conved = lax.all_to_all(result.astype(BF16), tp, split_axis=0, concat_axis=1, tiled=True)

    floats = conved.astype(F32)
    mean = jnp.mean(floats, axis=1, keepdims=True)
    spread = jnp.mean(floats * floats, axis=1, keepdims=True) - mean * mean
    activated = jax.nn.silu((floats - mean) * lax.rsqrt(spread + eps) * chan_gain + chan_shift).astype(BF16)
    projected = jnp.dot(activated, out_weight, preferred_element_type=F32)
    resid = (stream.astype(F32) + projected).astype(BF16)
    resid_float = resid.astype(F32)
    mean_square = jnp.mean(resid_float * resid_float, axis=-1, keepdims=True)
    normed = (resid_float * lax.rsqrt(mean_square + eps) * rms_gain).astype(BF16)

    local_experts = expert_gate.shape[0]
    experts_all = sp_count * local_experts
    top_count = expert_ids.shape[1]
    capacity = max(2, 3 * own_rows * top_count // (2 * experts_all))
    gap = route_logits[:, 0] - route_logits[:, 1]
    weights = [group_prob * jax.nn.sigmoid(gap), group_prob * jax.nn.sigmoid(-gap)]
    names = [
        (jnp.arange(experts_all, dtype=jnp.int32)[:, None] == expert_ids[:, k][None, :]).astype(F32)
        for k in range(top_count)
    ]
    named = sum(names)
    weighted = sum(n * w[None, :] for n, w in zip(names, weights))
    order = jnp.arange(own_rows, dtype=jnp.int32)
    before = (order[:, None] < order[None, :]).astype(BF16)
    ranks = jnp.dot(named.astype(BF16), before, preferred_element_type=F32)
    slots = jnp.arange(capacity, dtype=jnp.int32).astype(F32)
    picks = (ranks[:, None, :] == slots[None, :, None]) & (named[:, None, :] > 0)
    picks = picks.reshape(experts_all * capacity, own_rows)
    outgoing = jnp.dot(picks.astype(BF16), normed, preferred_element_type=F32).astype(BF16)
    outgoing = outgoing.reshape(experts_all, capacity, width)
    arrived = lax.all_to_all(outgoing, ("sp", "tx"), split_axis=0, concat_axis=0, tiled=True)
    rows = arrived.reshape(-1, width)
    total = None
    for gate, up, down in zip(gates_w, ups_w, downs_w):
        gated = jnp.dot(rows, gate, preferred_element_type=F32)
        upward = jnp.dot(rows, up, preferred_element_type=F32)
        hidden = (jax.nn.silu(gated) * upward).astype(BF16)
        part = jnp.dot(hidden, down, preferred_element_type=F32)
        total = part if total is None else total + part
    routed = lax.all_to_all(
        total.astype(BF16).reshape(arrived.shape), ("sp", "tx"), split_axis=0, concat_axis=0, tiled=True
    ).reshape(-1, width)
    spots = jnp.where(picks, jnp.repeat(weighted, capacity, axis=0), 0.0)
    high = spots.astype(BF16)
    low = (spots - high.astype(F32)).astype(BF16)
    both = jnp.concatenate([high, low], axis=1)
    mixed = lax.dot_general(both, routed, (((0,), (0,)), ((), ())), preferred_element_type=F32)
    return (resid_float + mixed[:own_rows] + mixed[own_rows:]).astype(BF16)


def solution(mesh):
    sp, tp = mesh.shape["sp"], mesh.shape["tp"]

    def whole(*args):
        nx = args[13].shape[0] // sp
        fine = Mesh(mesh.devices.reshape(sp, nx, tp // nx), ("sp", "tx", "tc"))
        t = ("tx", "tc")
        placed = (
            P(("sp",) + t, None), P("sp", t), P("sp", t), P("sp"), P(None, t), P(t), P(), P(), P(), P(),
            P(("sp",) + t, None), P(("sp",) + t), P(("sp",) + t, None),
            P("sp", None, t), P("sp", None, t), P("sp", t, None),
        )
        return jax.shard_map(
            body, mesh=fine, in_specs=placed, out_specs=P(("sp",) + t, None), check_vma=False
        )(*args)

    return whole
```

time: 322 us -> 191 us (0.59)
  blocking collectives: 123 us -> 0 us
  matrix products: 8.06 us -> 40.7 us
  local copies, waits for them, and re-layouts: 28.4 us -> 11.6 us
  other arithmetic: 22.6 us -> 8.05 us
  between operations: 13.7 us -> 0.34 us
  starting transfers between devices: 17.3 us -> 22.7 us
  waiting for transfers between devices: 109 us -> 105 us
    all_to_all x2 -> x0, blocking collectives: 117 us -> none  [the longest x1 74.2 us: body(): lax.all_to_all(split_quarters(partial_value, tp_count), 'tp', split_axis=...]
    ppermute x3 -> x10, waiting for transfers between devices: 0.01 us -> 66.3 us  [the longest x9 66.3 us: swap(): return lax.ppermute(x, axis, [(i, (i + by) % size) for i in range(size)])]
    all_gather x1 -> x0, waiting for transfers between devices: 44.6 us -> none  [body(): arrived = lax.all_gather(arrived_own, 'tp', axis=2, tiled=True)]
    dot_general x7 -> x12, matrix products: 8.06 us -> 40.7 us  [the longest x4 24.4 us: body(): part = jnp.dot(hidden, down, preferred_element_type=F32)]
    reduce_scatter x1 -> x0, waiting for transfers between devices: 27.7 us -> none  [body(): lax.psum_scatter(jnp.dot(activated, weight_rows, preferred_element_type=j...]
    reduce_sum x5 -> x1, other arithmetic: 15.7 us -> 0.12 us  [body(): mean = jnp.mean(floats, axis=1, keepdims=True)]
    all_to_all x1 -> x3, starting transfers between devices: 5.52 us -> 14.2 us  [the longest x1 5.78 us: body(): lax.all_to_all(total.astype(BF16).reshape(arrived.shape), ('sp', 'tx'), s...]
    gather x2 -> x0, local copies, waits for them, and re-layouts: 8.09 us -> none  [the longest x1 4.96 us: body(): flat_out[dest].reshape(own_rows, top_count, normed.shape[1])]
  transfers between devices with their start and end apart: 6 -> 13, of which waited for: 3 -> 5; matrix products, arithmetic and copies ran while one was open for 3% -> 19% of each run, Pallas kernels for 0% -> 0%
where the time goes in v1:
time: 191 us; the launch traced here: 188 us
  waiting for transfers between devices  105 us (55%)
  matrix products  40.7 us (21%)
  starting transfers between devices  22.7 us (12%)
  local copies, waits for them, and re-layouts  11.6 us (6%)
  other arithmetic  8.05 us (4%)
    ppermute x9, waiting for transfers between devices, swap(): return lax.ppermute(x, axis, [(i, (i + by) % size) for i in range(size)])  66.3 us
    all_to_all x1, waiting for transfers between devices, body(): lax.all_to_all(total.astype(BF16).reshape(arrived.shape), ('sp', 'tx'), s...  34 us
    dot_general x4, matrix products, body(): part = jnp.dot(hidden, down, preferred_element_type=F32)  24.4 us
    dot_general x4, matrix products, body(): gated = jnp.dot(rows, gate, preferred_element_type=F32)  10.6 us
    all_to_all x1, starting transfers between devices, body(): lax.all_to_all(total.astype(BF16).reshape(arrived.shape), ('sp', 'tx'), s...  5.78 us
    squeeze x3, local copies, waits for them, and re-layouts, gather_pieces(): lax.dynamic_index_in_dim(weight, lax.rem(me + by, nx), 0, keepdims=False)  5.74 us
    all_to_all x1, starting transfers between devices, body(): lax.all_to_all(outgoing, ('sp', 'tx'), split_axis=0, concat_axis=0, tiled...  5.04 us
    ppermute x1, starting transfers between devices, body(): tail = lax.ppermute(tail, 'sp', [(i, i + 1) for i in range(sp_count - 1)])  4.9 us
  transfers between devices with their start and end apart: 13, of which 5 were waited for; matrix products, arithmetic and copies ran while one was open for 19% of the time, Pallas kernels for 0%

profile of v1, /device:TPU:0, one launch (start us, length us, event | category | flops | bytes accessed | tf_op | source)
XLA Modules:
  0.0 188.1 jit_solution(5941658325924492186)
XLA Ops:
  0.0 0.9 slice.313
  0.9 0.7 slice.312
  1.6 0.7 fusion.104
  2.2 0.1 slice.314
  2.3 0.1 pad.10.clone
  2.4 0.1 maximum_maximum_fusion
  2.5 4.9 %collective-permute-start = (bf16[90,128]{1,0:T(8,128)(2,1)S(1)}, bf16[90,128]{1,0:T(8,128)(2,1)S(1)}, u32[]{:S(2)}, u32[]{:S(2)}) collective-permute-start(bf16[90,128]{1,0:T(8,128)(2,1)S(1)} %maximum_maximum_fusion), channel_id=1, source_target_pairs={{0,4},{4,8},{8,12},{12,16},{16,20},{20,24},{24,28},{1,5},{5,9},{9,... | collective-permute-start | bytes 69128 | tf_op jit(solution)/shard_map/ppermute | solution.py:38
  7.4 1.0 slice_bitcast_fusion.31
  8.3 1.0 slice_bitcast_fusion.32
  9.4 0.8 slice_bitcast_fusion.1
  10.1 0.1 fusion.93
  10.3 0.0 collective-permute-done
  10.3 0.4 copy-done.5
  10.7 0.1 slice_reduce_fusion
  10.8 0.1 pad_maximum_fusion
  10.8 0.1 slice_compare_fusion.28
  10.9 0.1 slice_compare_fusion.29
  11.1 1.1 divide_multiply_fusion
  12.2 0.0 copy-start.9
  12.2 0.0 copy-start.10
  12.2 4.2 %fusion.15 = bf16[512,128]{1,0:T(8,128)(2,1)} fusion(f32[542,128]{1,0:T(8,128)S(1)} %divide_multiply_fusion, f32[128]{0:T(128)S(1)} %get-tuple-element.46, f32[128]{0:T(128)S(1)} %get-tuple-element.47, f32[128]{0:T(128)S(1)} %get-tuple-element.18, f32[128]{0:T(128)S(1)} %get-tuple-element.19, f32[128]{0:T(128)S(1)} %get-tuple-element.20, ...), kind=kLoop, calls=%fused_computation.37 | loop fusion | flops 6160384 | bytes 8289792 | tf_op jit(solution)/shard_map/convert_element_type | solution.py:50
  16.3 3.3 %all-to-all-start = ((bf16[4,128,128]{2,1,0:T(8,128)(2,1)}), bf16[4,128,128]{2,1,0:T(8,128)(2,1)S(1)}, u32[]{:S(2)}, u32[]{:S(2)}) async-start(bf16[4,128,128]{2,1,0:T(8,128)(2,1)} %bitcast.31), calls=%async_computation | async-start | bytes 262144 | tf_op jit(solution)/shard_map/all_to_all | solution.py:50
  19.7 0.1 eq.193
  19.8 0.1 fusion.92
  19.9 4.3 %all-to-all-done = bf16[4,128,128]{2,1,0:T(8,128)(2,1)S(1)} async-done(((bf16[4,128,128]{2,1,0:T(8,128)(2,1)}), bf16[4,128,128]{2,1,0:T(8,128)(2,1)S(1)}, u32[]{:S(2)}, u32[]{:S(2)}) %all-to-all-start) | async-done | bytes 131104 | tf_op jit(solution)/shard_map/all_to_all | solution.py:50
  24.3 0.1 copy.17
  24.4 0.1 convert_reduce_fusion
  24.5 0.2 multiply_convert_fusion.5
  24.8 0.0 copy-start.4
  24.8 1.6 multiply_reduce_fusion
  26.4 1.8 convolution_convert_fusion
  28.3 5.0 %all-to-all-start.1 = ((bf16[16,24,2048]{2,1,0:T(8,128)(2,1)}), bf16[16,24,2048]{2,1,0:T(8,128)(2,1)}, u32[]{:S(2)}, u32[]{:S(2)}) async-start(bf16[16,24,2048]{2,1,0:T(8,128)(2,1)} %bitcast.147), calls=%async_computation.1 | async-start | bytes 3145728 | tf_op jit(solution)/shard_map/all_to_all | solution.py:82
  33.3 0.0 copy-start.1
  33.3 2.8 %dynamic-slice_bitcast_fusion.2 = (bf16[2048,256]{1,0:T(8,128)(2,1)S(1)}, bf16[2048,256]{1,0:T(8,128)(2,1)}) fusion(bf16[2,2048,256]{2,1,0:T(8,128)(2,1)} %param.29, s32[]{:T(128)S(6)} %select_n.143, s32[]{:T(128)S(6)} %select_n.142), kind=kLoop, calls=%fused_computation.13 | loop fusion | bytes 4194312 | tf_op jit(solution)/shard_map/jit(dynamic_index_in_dim)/squeeze | solution.py:20
  36.1 1.9 collective-permute-start.1
  38.0 1.5 dynamic-slice_bitcast_fusion
  39.5 0.2 collective-permute-start.3
  39.6 0.7 copy-done.2
  40.3 1.5 dynamic-slice_bitcast_fusion.1
  41.8 1.1 collective-permute-start.2
  43.0 33.3 %collective-permute-done.1 = bf16[2048,256]{1,0:T(8,128)(2,1)} collective-permute-done((bf16[2048,256]{1,0:T(8,128)(2,1)S(1)}, bf16[2048,256]{1,0:T(8,128)(2,1)}, u32[]{:S(2)}, u32[]{:S(2)}) %collective-permute-start.1) | collective-permute-done | bytes 1048608 | tf_op jit(solution)/shard_map/ppermute | solution.py:12
  76.3 0.0 collective-permute-start.7
  76.3 0.0 all-to-all-done.1
  76.3 2.3 %fusion.112 = f32[384,256]{1,0:T(8,128)S(1)} fusion(bf16[384,2048]{1,0:T(8,128)(2,1)} %bitcast.42, bf16[2048,256]{1,0:T(8,128)(2,1)} %get-tuple-element.10), kind=kOutput, calls=%fused_computation.242 | convolution fusion | flops 402653184 | bytes 3014656 | tf_op jit(solution)/shard_map/dot_general | solution.py:86
  78.5 5.4 %fusion.3 = f32[384,2048]{1,0:T(8,128)} fusion(bf16[256,2048]{1,0:T(8,128)(2,1)} %get-tuple-element.14, bf16[384,2048]{1,0:T(8,128)(2,1)} %bitcast.42, bf16[2048,256]{1,0:T(8,128)(2,1)} %get-tuple-element.12, f32[384,256]{1,0:T(8,128)S(1)} %fusion.112), kind=kOutput, calls=%fused_computation.7 | convolution fusion | flops 805896192 | bytes 7208960 | tf_op jit(solution)/shard_map/dot_general | solution.py:89
  84.0 0.5 collective-permute-start.5
  84.5 2.3 %fusion.113 = f32[384,256]{1,0:T(8,128)S(1)} fusion(bf16[384,2048]{1,0:T(8,128)(2,1)} %bitcast.42, bf16[2048,256]{1,0:T(8,128)(2,1)} %collective-permute-done.1), kind=kOutput, calls=%fused_computation.243 | convolution fusion | flops 402653184 | bytes 3014656 | tf_op jit(solution)/shard_map/dot_general | solution.py:86
  86.8 11.9 %collective-permute-done.3 = bf16[256,2048]{1,0:T(8,128)(2,1)} collective-permute-done((bf16[256,2048]{1,0:T(8,128)(2,1)}, bf16[256,2048]{1,0:T(8,128)(2,1)}, u32[]{:S(2)}, u32[]{:S(2)}) %collective-permute-start.3) | collective-permute-done | bytes 1048608 | tf_op jit(solution)/shard_map/ppermute | solution.py:12
  98.7 0.0 collective-permute-start.9
  98.7 21.0 %collective-permute-done.2 = bf16[2048,256]{1,0:T(8,128)(2,1)} collective-permute-done((bf16[2048,256]{1,0:T(8,128)(2,1)}, bf16[2048,256]{1,0:T(8,128)(2,1)}, u32[]{:S(2)}, u32[]{:S(2)}) %collective-permute-start.2) | collective-permute-done | bytes 1048608 | tf_op jit(solution)/shard_map/ppermute | solution.py:12
  119.8 0.0 collective-permute-start.8
  119.8 3.0 %fusion.114 = f32[384,256]{1,0:T(8,128)} fusion(bf16[384,2048]{1,0:T(8,128)(2,1)} %bitcast.42, bf16[2048,256]{1,0:T(8,128)(2,1)} %collective-permute-done.4), kind=kOutput, calls=%fused_computation.244 | convolution fusion | flops 402653184 | bytes 3014656 | tf_op jit(solution)/shard_map/dot_general | solution.py:86
  122.8 3.0 %fusion.115 = f32[384,256]{1,0:T(8,128)} fusion(bf16[384,2048]{1,0:T(8,128)(2,1)} %bitcast.42, bf16[2048,256]{1,0:T(8,128)(2,1)} %collective-permute-done.7), kind=kOutput, calls=%fused_computation.245 | convolution fusion | flops 402653184 | bytes 3014656 | tf_op jit(solution)/shard_map/dot_general | solution.py:86
  125.8 5.5 %fusion.79 = f32[384,2048]{1,0:T(8,128)} fusion(bf16[256,2048]{1,0:T(8,128)(2,1)} %collective-permute-done.3, f32[384,256]{1,0:T(8,128)S(1)} %fusion.113, bf16[384,2048]{1,0:T(8,128)(2,1)} %bitcast.42, bf16[2048,256]{1,0:T(8,128)(2,1)} %collective-permute-done.2), kind=kOutput, calls=%fused_computation.133 | convolution fusion | flops 805896192 | bytes 7208960 | tf_op jit(solution)/shard_map/dot_general | solution.py:89
  131.3 0.0 collective-permute-done.6
  131.3 0.0 collective-permute-done.5
  131.3 5.7 %fusion.80 = f32[384,2048]{1,0:T(8,128)} fusion(bf16[256,2048]{1,0:T(8,128)(2,1)} %collective-permute-done.6, f32[384,256]{1,0:T(8,128)} %fusion.114, bf16[384,2048]{1,0:T(8,128)(2,1)} %bitcast.42, bf16[2048,256]{1,0:T(8,128)(2,1)} %collective-permute-done.5), kind=kOutput, calls=%fused_computation.134 | convolution fusion | flops 805896192 | bytes 7208960 | tf_op jit(solution)/shard_map/dot_general | solution.py:89
  137.0 7.8 %add_convert_fusion = bf16[384,2048]{1,0:T(8,128)(2,1)} fusion(f32[384,2048]{1,0:T(8,128)} %fusion.80, f32[384,2048]{1,0:T(8,128)} %fusion.3, f32[384,2048]{1,0:T(8,128)} %fusion.79, bf16[256,2048]{1,0:T(8,128)(2,1)} %collective-permute-done.9, f32[384,256]{1,0:T(8,128)S(1)} %copy-done.3, bf16[384,2048]{1,0:T(8,128)(2,1)} %bitcast.42, ...), kind=kOutput, calls=%fused_computation | convolution fusion | flops 809041920 | bytes 15073280 | tf_op jit(solution)/shard_map/dot_general | solution.py:89
  144.9 5.8 %all-to-all-start.2 = ((bf16[16,24,2048]{2,1,0:T(8,128)(2,1)}), bf16[16,24,2048]{2,1,0:T(8,128)(2,1)}, u32[]{:S(2)}, u32[]{:S(2)}) async-start(bf16[16,24,2048]{2,1,0:T(8,128)(2,1)} %bitcast.148), calls=%async_computation.2 | async-start | bytes 3145728 | tf_op jit(solution)/shard_map/all_to_all | solution.py:91
  150.7 0.1 fusion.87
  150.8 0.1 fusion.86
  151.0 34.0 %all-to-all-done.2 = bf16[16,24,2048]{2,1,0:T(8,128)(2,1)} async-done(((bf16[16,24,2048]{2,1,0:T(8,128)(2,1)}), bf16[16,24,2048]{2,1,0:T(8,128)(2,1)}, u32[]{:S(2)}, u32[]{:S(2)}) %all-to-all-start.2) | async-done | bytes 1572896 | tf_op jit(solution)/shard_map/all_to_all | solution.py:91
  185.0 2.1 %fusion.81 = f32[256,2048]{1,0:T(8,128)S(1)} fusion(bf16[384,2048]{1,0:T(8,128)(2,1)} %bitcast.50, bf16[384,128]{1,0:T(8,128)(2,1)S(1)} %fusion.87, bf16[384,128]{1,0:T(8,128)(2,1)S(1)} %fusion.86), kind=kOutput, calls=%fused_computation.135 | convolution fusion | flops 403046400 | bytes 3866624 | tf_op jit(solution)/shard_map/dot_general | solution.py:98
  187.1 1.0 fusion.4
  (35 shorter events, 0.1 us)
Async XLA Ops:
  0.0 24.8 %copy-start = (bf16[512,2048]{1,0:T(8,128)(2,1)S(1)}, bf16[512,2048]{1,0:T(8,128)(2,1)}, u32[]{:S(2)}) copy-start(bf16[512,2048]{1,0:T(8,128)(2,1)} %param.24) | copy-start | bytes 6291460
  2.5 7.8 %collective-permute-start = (bf16[90,128]{1,0:T(8,128)(2,1)S(1)}, bf16[90,128]{1,0:T(8,128)(2,1)S(1)}, u32[]{:S(2)}, u32[]{:S(2)}) collective-permute-start(bf16[90,128]{1,0:T(8,128)(2,1)S(1)} %maximum_maximum_fusion), channel_id=1, source_target_pairs={{0,4},{4,8},{8,12},{12,16},{16,20},{20,24},{24,28},{1,5},{5,9},{9,... | collective-permute-start | bytes 69128 | tf_op jit(solution)/shard_map/ppermute | solution.py:38
  10.1 0.5 copy-start.5
  10.1 0.9 copy-start.7
  12.2 12.4 %copy-start.9 = (f32[512]{0:T(512)S(1)}, f32[512]{0:T(512)}, u32[]{:S(2)}) copy-start(f32[512]{0:T(512)} %param.23) | copy-start | bytes 6148
  12.2 12.4 %copy-start.10 = (f32[512]{0:T(512)S(1)}, f32[512]{0:T(512)}, u32[]{:S(2)}) copy-start(f32[512]{0:T(512)} %param.22) | copy-start | bytes 6148
  16.3 7.9 %all-to-all-start = ((bf16[4,128,128]{2,1,0:T(8,128)(2,1)}), bf16[4,128,128]{2,1,0:T(8,128)(2,1)S(1)}, u32[]{:S(2)}, u32[]{:S(2)}) async-start(bf16[4,128,128]{2,1,0:T(8,128)(2,1)} %bitcast.31), calls=%async_computation | async-start | bytes 262144 | tf_op jit(solution)/shard_map/all_to_all | solution.py:50
  24.8 1.6 copy-start.4
  28.3 48.0 %all-to-all-start.1 = ((bf16[16,24,2048]{2,1,0:T(8,128)(2,1)}), bf16[16,24,2048]{2,1,0:T(8,128)(2,1)}, u32[]{:S(2)}, u32[]{:S(2)}) async-start(bf16[16,24,2048]{2,1,0:T(8,128)(2,1)} %bitcast.147), calls=%async_computation.1 | async-start | bytes 3145728 | tf_op jit(solution)/shard_map/all_to_all | solution.py:82
  33.3 4.7 %copy-start.1 = (bf16[2,256,2048]{2,1,0:T(8,128)(2,1)S(1)}, bf16[2,256,2048]{2,1,0:T(8,128)(2,1)}, u32[]{:S(2)}) copy-start(bf16[2,256,2048]{2,1,0:T(8,128)(2,1)} %param.31) | copy-start | bytes 6291460
  36.1 40.1 %collective-permute-start.1 = (bf16[2048,256]{1,0:T(8,128)(2,1)S(1)}, bf16[2048,256]{1,0:T(8,128)(2,1)}, u32[]{:S(2)}, u32[]{:S(2)}) collective-permute-start(bf16[2048,256]{1,0:T(8,128)(2,1)S(1)} %get-tuple-element.9), channel_id=1, source_target_pairs={{0,2},{2,0},{1,3},{3,1},{4,6},{6,4},{5,7},{7,5},{8,10},{10,8},{9,1... | collective-permute-start | bytes 3145736 | tf_op jit(solution)/shard_map/ppermute | solution.py:12
  38.0 2.3 %copy-start.2 = (bf16[2,2048,256]{2,1,0:T(8,128)(2,1)S(1)}, bf16[2,2048,256]{2,1,0:T(8,128)(2,1)}, u32[]{:S(2)}) copy-start(bf16[2,2048,256]{2,1,0:T(8,128)(2,1)} %param.30) | copy-start | bytes 6291460
  38.0 46.0 %collective-permute-start.4 = (bf16[2048,256]{1,0:T(8,128)(2,1)}, bf16[2048,256]{1,0:T(8,128)(2,1)}, u32[]{:S(2)}, u32[]{:S(2)}) collective-permute-start(bf16[2048,256]{1,0:T(8,128)(2,1)} %get-tuple-element.10), channel_id=1, source_target_pairs={{0,1},{1,0},{2,3},{3,2},{4,5},{5,4},{6,7},{7,6},{8,9},{9,8},{10,11... | collective-permute-start | bytes 3145736 | tf_op jit(solution)/shard_map/ppermute | solution.py:12
  39.5 59.3 %collective-permute-start.3 = (bf16[256,2048]{1,0:T(8,128)(2,1)}, bf16[256,2048]{1,0:T(8,128)(2,1)}, u32[]{:S(2)}, u32[]{:S(2)}) collective-permute-start(bf16[256,2048]{1,0:T(8,128)(2,1)} %get-tuple-element.13), channel_id=1, source_target_pairs={{0,2},{2,0},{1,3},{3,1},{4,6},{6,4},{5,7},{7,5},{8,10},{10,8},{9,1... | collective-permute-start | bytes 3145736 | tf_op jit(solution)/shard_map/ppermute | solution.py:12
  41.8 78.0 %collective-permute-start.2 = (bf16[2048,256]{1,0:T(8,128)(2,1)}, bf16[2048,256]{1,0:T(8,128)(2,1)}, u32[]{:S(2)}, u32[]{:S(2)}) collective-permute-start(bf16[2048,256]{1,0:T(8,128)(2,1)} %get-tuple-element.11), channel_id=1, source_target_pairs={{0,2},{2,0},{1,3},{3,1},{4,6},{6,4},{5,7},{7,5},{8,10},{10,8},{9,1... | collective-permute-start | bytes 3145736 | tf_op jit(solution)/shard_map/ppermute | solution.py:12
  43.0 88.4 %collective-permute-start.6 = (bf16[256,2048]{1,0:T(8,128)(2,1)}, bf16[256,2048]{1,0:T(8,128)(2,1)}, u32[]{:S(2)}, u32[]{:S(2)}) collective-permute-start(bf16[256,2048]{1,0:T(8,128)(2,1)} %get-tuple-element.14), channel_id=1, source_target_pairs={{0,1},{1,0},{2,3},{3,2},{4,5},{5,4},{6,7},{7,6},{8,9},{9,8},{10,11... | collective-permute-start | bytes 3145736 | tf_op jit(solution)/shard_map/ppermute | solution.py:12
  76.3 46.5 %collective-permute-start.7 = (bf16[2048,256]{1,0:T(8,128)(2,1)}, bf16[2048,256]{1,0:T(8,128)(2,1)}, u32[]{:S(2)}, u32[]{:S(2)}) collective-permute-start(bf16[2048,256]{1,0:T(8,128)(2,1)} %collective-permute-done.1), channel_id=1, source_target_pairs={{0,1},{1,0},{2,3},{3,2},{4,5},{5,4},{6,7},{7,6},{8,9},{9,8},{10,11... | collective-permute-start | bytes 3145736 | tf_op jit(solution)/shard_map/ppermute | solution.py:12
  84.0 47.3 %collective-permute-start.5 = (bf16[2048,256]{1,0:T(8,128)(2,1)}, bf16[2048,256]{1,0:T(8,128)(2,1)}, u32[]{:S(2)}, u32[]{:S(2)}) collective-permute-start(bf16[2048,256]{1,0:T(8,128)(2,1)} %get-tuple-element.12), channel_id=1, source_target_pairs={{0,1},{1,0},{2,3},{3,2},{4,5},{5,4},{6,7},{7,6},{8,9},{9,8},{10,11... | collective-permute-start | bytes 3145736 | tf_op jit(solution)/shard_map/ppermute | solution.py:12
  98.7 38.3 %collective-permute-start.9 = (bf16[256,2048]{1,0:T(8,128)(2,1)}, bf16[256,2048]{1,0:T(8,128)(2,1)}, u32[]{:S(2)}, u32[]{:S(2)}) collective-permute-start(bf16[256,2048]{1,0:T(8,128)(2,1)} %collective-permute-done.3), channel_id=1, source_target_pairs={{0,1},{1,0},{2,3},{3,2},{4,5},{5,4},{6,7},{7,6},{8,9},{9,8},{10,11... | collective-permute-start | bytes 3145736 | tf_op jit(solution)/shard_map/ppermute | solution.py:12
  119.8 17.2 %collective-permute-start.8 = (bf16[2048,256]{1,0:T(8,128)(2,1)}, bf16[2048,256]{1,0:T(8,128)(2,1)}, u32[]{:S(2)}, u32[]{:S(2)}) collective-permute-start(bf16[2048,256]{1,0:T(8,128)(2,1)} %collective-permute-done.2), channel_id=1, source_target_pairs={{0,1},{1,0},{2,3},{3,2},{4,5},{5,4},{6,7},{7,6},{8,9},{9,8},{10,11... | collective-permute-start | bytes 3145736 | tf_op jit(solution)/shard_map/ppermute | solution.py:12
  131.3 5.7 %copy-start.3 = (f32[384,256]{1,0:T(8,128)S(1)}, f32[384,256]{1,0:T(8,128)}, u32[]{:S(2)}) copy-start(f32[384,256]{1,0:T(8,128)} %fusion.115) | copy-start | bytes 1179652
  144.8 5.8 %copy-start.11 = (f32[128,2]{0,1:T(2,128)S(1)}, f32[128,2]{0,1:T(2,128)}, u32[]{:S(2)}) copy-start(f32[128,2]{0,1:T(2,128)} %param.28) | copy-start | bytes 3076
  144.8 5.8 %copy-start.12 = (f32[128]{0:T(128)S(1)}, f32[128]{0:T(128)}, u32[]{:S(2)}) copy-start(f32[128]{0:T(128)} %param.27) | copy-start | bytes 1540
  144.8 5.8 %copy-start.6 = (s32[128]{0:T(128)S(1)}, s32[128]{0:T(128)}, u32[]{:S(2)}) copy-start(s32[128]{0:T(128)} %copy-done.5) | copy-start | bytes 1540
  144.8 5.9 %copy-start.8 = (s32[128]{0:T(128)S(1)}, s32[128]{0:T(128)}, u32[]{:S(2)}) copy-start(s32[128]{0:T(128)} %copy-done.7) | copy-start | bytes 1540
  144.9 40.1 %all-to-all-start.2 = ((bf16[16,24,2048]{2,1,0:T(8,128)(2,1)}), bf16[16,24,2048]{2,1,0:T(8,128)(2,1)}, u32[]{:S(2)}, u32[]{:S(2)}) async-start(bf16[16,24,2048]{2,1,0:T(8,128)(2,1)} %bitcast.148), calls=%async_computation.2 | async-start | bytes 3145728 | tf_op jit(solution)/shard_map/all_to_all | solution.py:91

commit v2 on v1

v2 whole, which is shorter than its diff:
```python
import functools

import jax
import jax.numpy as jnp
from jax import lax
from jax.experimental import pallas as pl
from jax.experimental.pallas import tpu as pltpu
from jax.sharding import PartitionSpec as P

eps = 1e-06
F32, BF16 = jnp.float32, jnp.bfloat16
MESH = pl.DeviceIdType.MESH


def flipped(index, mask):
    bit = 1
    while bit <= mask:
        if mask & bit:
            index = index + bit * (1 - 2 * lax.rem(lax.div(index, bit), 2))
        bit *= 2
    return index


def exchange_kernel(
    sp, local, slab_rows, groups,
    out_ref, gate_ref, up_ref, down_ref, ret_ref,
    rows, x_buf, hid_buf, own, part_send, part_recv, back, wg, wu, wd,
    disp_sems, relay_sems, part_sems, back_sems, weight_sems, fetch_sems,
):
    s, t = lax.axis_index("sp"), lax.axis_index("tp")
    h, l = lax.div(t, local), lax.rem(t, local)
    half = slab_rows // 2
    across = (s, (1 - h) * local + l)
    count = sp * local
    own_expert = s * local + l

    def peer(slot):
        m, dl = divmod(slot, local)
        return flipped(s, m), flipped(l, dl)

    def device(slot):
        ps, plocal = peer(slot)
        return (ps, h * local + plocal)

    def remote(src, dst, sems, slot, where):
        return pltpu.make_async_remote_copy(
            src_ref=src, dst_ref=dst, send_sem=sems.at[0, slot], recv_sem=sems.at[1, slot],
            device_id=where, device_id_type=MESH,
        )

    barrier = pltpu.get_barrier_semaphore()
    for slot in range(1, count):
        pl.semaphore_signal(barrier, inc=1, device_id=device(slot), device_id_type=MESH)
    pl.semaphore_signal(barrier, inc=1, device_id=across, device_id_type=MESH)
    pl.semaphore_wait(barrier, count)

    relay, part, back_copies = {}, {}, {}
    dispatch = {}
    for first, last in groups[1:] + groups[:1]:
        for slot in range(first, last):
            if slot:
                ps, plocal = peer(slot)
                dispatch[slot] = remote(
                    out_ref.at[ps * local + plocal], rows.at[0, slot], disp_sems, slot, device(slot)
                )
                dispatch[slot].start()
    relay[0] = remote(out_ref.at[own_expert], rows.at[1, 0], relay_sems, 0, across)
    relay[0].start()
    weights, fetches = [], []
    for k, (src, dst) in enumerate(((gate_ref, wg), (up_ref, wu), (down_ref, wd))):
        fetch = pltpu.make_async_copy(src.at[l], dst.at[0], fetch_sems.at[k])
        fetch.start()
        fetches.append(fetch)
        for dl in range(1, local):
            copy = remote(
                src.at[flipped(l, dl)], dst.at[dl], weight_sems, k * local + dl, (s, h * local + flipped(l, dl))
            )
            copy.start()
            weights.append(copy)
    rows[0, 0] = out_ref[own_expert]

    def pass_across(g):
        for slot in range(*groups[g]):
            if slot:
                dispatch[slot].wait_recv()
                relay[slot] = remote(rows.at[0, slot], rows.at[1, slot], relay_sems, slot, across)
                relay[slot].start()

    size = (groups[0][1] - groups[0][0]) * half
    deep = out_ref.shape[2]

    def compute(g):
        first, last = groups[g]
        for slot in range(first, last):
            relay[slot].wait_recv()
        for plane in range(2):
            slabs = rows[plane, first:last].astype(F32)
            for side in range(2):
                x_buf[plane * size : (plane + 1) * size, side * deep : (side + 1) * deep] = (
                    slabs[:, side * half : (side + 1) * half].reshape(size, deep).astype(BF16)
                )
        for dl in range(local):
            x = x_buf[...]
            gated = jnp.dot(x, wg[dl], preferred_element_type=F32)
            upward = jnp.dot(x, wu[dl], preferred_element_type=F32)
            hid_buf[dl] = (jax.nn.silu(gated) * upward).astype(BF16)
        step = min(256, deep)

        for at in range(0, deep, step):
            sides = []
            for side in range(2):
                total = None
                for dl in range(local):
                    term = jnp.dot(
                        hid_buf[dl], wd[dl, :, side * deep + at : side * deep + at + step],
                        preferred_element_type=F32,
                    )
                    total = term if total is None else total + term
                sides.append(total.reshape(2, last - first, half, step))
            slabs = jnp.concatenate(sides, axis=2)
            own[first:last, :, at : at + step] = slabs[0]
            part_send[first:last, :, at : at + step] = slabs[1].astype(BF16)
        for slot in range(first, last):
            part[slot] = remote(part_send.at[slot], part_recv.at[slot], part_sems, slot, across)
            part[slot].start()

    def finish(g):
        for slot in range(*groups[g]):
            part[slot].wait_recv()
            total = (own[slot] + part_recv[slot].astype(F32)).astype(BF16)
            if slot == 0:
                ret_ref[own_expert] = total
            else:
                back[slot] = total
                back_copies[slot] = remote(back.at[slot], ret_ref.at[own_expert], back_sems, slot, device(slot))
                back_copies[slot].start()

    pass_across(0)
    for copy in fetches:
        copy.wait()
    for copy in weights:
        copy.wait_recv()
    amount = len(groups)
    for g in range(amount + 2):
        if 1 <= g < amount:
            pass_across(g)
        if 1 <= g <= amount:
            compute(g - 1)
        if g >= 2:
            finish(g - 2)
    for slot in range(1, count):
        back_copies[slot].wait_recv()
    for copies in (dispatch, relay, part, back_copies):
        for copy in copies.values():
            copy.wait_send()
    for copy in weights:
        copy.wait_send()


def run_experts(outgoing, expert_gate, expert_up, expert_down):
    sp = lax.axis_size("sp")
    count, slab_rows, deep = outgoing.shape
    local = expert_gate.shape[0]
    quarter = count // 4
    groups = [(0, quarter), (2 * quarter, 3 * quarter), (quarter, 2 * quarter), (3 * quarter, count)]
    slabs = (count, slab_rows, deep)
    m = quarter * slab_rows
    sems = pltpu.SemaphoreType.DMA((2, count))
    return pl.pallas_call(
        functools.partial(exchange_kernel, sp, local, slab_rows, groups),
        out_shape=jax.ShapeDtypeStruct(slabs, BF16),
        in_specs=[pl.BlockSpec(memory_space=pltpu.VMEM)] + [pl.BlockSpec(memory_space=pl.ANY)] * 3,
        out_specs=pl.BlockSpec(memory_space=pltpu.VMEM),
        scratch_shapes=[
            pltpu.VMEM((2,) + slabs, BF16),
            pltpu.VMEM((m, 2 * deep), BF16),
            pltpu.VMEM((local, m, expert_gate.shape[2]), BF16),
            pltpu.VMEM(slabs, F32),
            pltpu.VMEM(slabs, BF16),
            pltpu.VMEM(slabs, BF16),
            pltpu.VMEM(slabs, BF16),
            pltpu.VMEM(expert_gate.shape, BF16),
            pltpu.VMEM(expert_up.shape, BF16),
            pltpu.VMEM(expert_down.shape, BF16),
            sems, sems, sems, sems,
            pltpu.SemaphoreType.DMA((2, 3 * local)),
            pltpu.SemaphoreType.DMA((3,)),
        ],
        compiler_params=pltpu.CompilerParams(
            collective_id=0, has_side_effects=True, vmem_limit_bytes=60 * 1024 * 1024
        ),
    )(outgoing, expert_gate, expert_up, expert_down)


def body(
    stream, conv_value, conv_gate, doc_ids, conv_taps, conv_bias, chan_gain, chan_shift, out_weight,
    rms_gain, expert_ids, group_prob, route_logits, expert_gate, expert_up, expert_down,
):
    reach = conv_taps.shape[0] - 1
    tp = "tp"
    own_rows, width = stream.shape
    sp_count = lax.axis_size("sp")
    block, chans = conv_value.shape
    docs_row = doc_ids.astype(BF16)
    tail = jnp.concatenate(
        [conv_value[-reach:], conv_gate[-reach:], jnp.broadcast_to(docs_row[-reach:, None], (reach, chans))], axis=0
    )
    tail = lax.ppermute(tail, "sp", [(i, i + 1) for i in range(sp_count - 1)])

    values = jnp.concatenate([tail[:reach], conv_value], axis=0).astype(F32)
    gates = jnp.concatenate([tail[reach : 2 * reach], conv_gate], axis=0).astype(F32)
    docs = jnp.concatenate([tail[2 * reach :, 0], docs_row], axis=0)
    acts = values * jax.nn.sigmoid(gates)
    result = jnp.broadcast_to(conv_bias[None, :], (block, chans))
    for offset in range(reach + 1):
        begin = reach - offset
        same = (docs[begin : begin + block] == docs_row)[:, None]
        result = result + jnp.where(same, acts[begin : begin + block], 0.0) * conv_taps[offset][None, :]
    conved = lax.all_to_all(result.astype(BF16), tp, split_axis=0, concat_axis=1, tiled=True)

    floats = conved.astype(F32)
    mean = jnp.mean(floats, axis=1, keepdims=True)
    spread = jnp.mean(floats * floats, axis=1, keepdims=True) - mean * mean
    activated = jax.nn.silu((floats - mean) * lax.rsqrt(spread + eps) * chan_gain + chan_shift).astype(BF16)
    projected = jnp.dot(activated, out_weight, preferred_element_type=F32)
    resid = (stream.astype(F32) + projected).astype(BF16)
    resid_float = resid.astype(F32)
    mean_square = jnp.mean(resid_float * resid_float, axis=-1, keepdims=True)
    normed = (resid_float * lax.rsqrt(mean_square + eps) * rms_gain).astype(BF16)

    local_experts = expert_gate.shape[0]
    experts_all = sp_count * local_experts
    top_count = expert_ids.shape[1]
    capacity = max(2, 3 * own_rows * top_count // (2 * experts_all))
    capacity = (capacity + 7) // 8 * 8
    gap = route_logits[:, 0] - route_logits[:, 1]
    weights = [group_prob * jax.nn.sigmoid(gap), group_prob * jax.nn.sigmoid(-gap)]
    names = [
        (jnp.arange(experts_all, dtype=jnp.int32)[:, None] == expert_ids[:, k][None, :]).astype(F32)
        for k in range(top_count)
    ]
    named = sum(names)
    weighted = sum(n * w[None, :] for n, w in zip(names, weights))
    order = jnp.arange(own_rows, dtype=jnp.int32)
    before = (order[:, None] < order[None, :]).astype(BF16)
    ranks = jnp.dot(named.astype(BF16), before, preferred_element_type=F32)
    slots = jnp.arange(capacity, dtype=jnp.int32).astype(F32)
    picks = (ranks[:, None, :] == slots[None, :, None]) & (named[:, None, :] > 0)
    side = jnp.eye(2, dtype=jnp.bool_)[None, :, None, :, None]
    picks = (picks[:, None, :, None, :] & side).reshape(experts_all * 2 * capacity, 2 * own_rows)
    halves = jnp.concatenate([normed[:, : width // 2], normed[:, width // 2 :]], axis=0)
    outgoing = jnp.dot(picks.astype(BF16), halves, preferred_element_type=F32).astype(BF16)
    outgoing = outgoing.reshape(experts_all, 2 * capacity, width // 2)
    routed = run_experts(outgoing, expert_gate, expert_up, expert_down).reshape(-1, width // 2)
    spread_weights = jnp.tile(jnp.repeat(weighted, 2 * capacity, axis=0), (1, 2))
    spots = jnp.where(picks, spread_weights, 0.0)
    high = spots.astype(BF16)
    low = (spots - high.astype(F32)).astype(BF16)
    both = jnp.concatenate([high, low], axis=1)
    mixed = lax.dot_general(both, routed, (((0,), (0,)), ((), ())), preferred_element_type=F32)
    mixed = mixed[: 2 * own_rows] + mixed[2 * own_rows :]
    mixed = jnp.concatenate([mixed[:own_rows], mixed[own_rows:]], axis=1)
    return (resid_float + mixed).astype(BF16)


def solution(mesh):
    placed = (
        P(("sp", "tp"), None), P("sp", "tp"), P("sp", "tp"), P("sp"), P(None, "tp"), P("tp"),
        P(), P(), P(), P(), P(("sp", "tp"), None), P(("sp", "tp")), P(("sp", "tp"), None),
        P("sp", None, "tp"), P("sp", None, "tp"), P("sp", "tp", None),
    )
    return jax.shard_map(
        body, mesh=mesh, in_specs=placed, out_specs=P(("sp", "tp"), None), check_vma=False
    )
```

time: 191 us -> 120 us (0.63); the launches traced: 188 us -> 120 us
  waiting for transfers between devices: 105 us -> 3.65 us
  Pallas kernels: 0 us -> 86.8 us
  matrix products: 40.7 us -> 5.85 us
  starting transfers between devices: 22.7 us -> 8.36 us
  local copies, waits for them, and re-layouts: 11.6 us -> 4.99 us
    pallas_call x0 -> x1, Pallas kernels: none -> 86.8 us  [run_experts(): pl.pallas_call(functools.partial(exchange_kernel, sp, local, slab_rows, g...]
    ppermute x9 -> x0, waiting for transfers between devices: 66.3 us -> none  [swap(): return lax.ppermute(x, axis, [(i, (i + by) % size) for i in range(size)])]
    dot_general x9 -> x1, matrix products: 36.9 us -> 1.72 us  [body(): jnp.dot(picks.astype(BF16), halves, preferred_element_type=F32).astype(BF16)]
    all_to_all x2 -> x0, waiting for transfers between devices: 34 us -> none  [the longest x1 34 us: body(): lax.all_to_all(total.astype(BF16).reshape(arrived.shape), ('sp', 'tx'), s...]
    all_to_all x2 -> x0, starting transfers between devices: 10.8 us -> none  [the longest x1 5.78 us: body(): lax.all_to_all(total.astype(BF16).reshape(arrived.shape), ('sp', 'tx'), s...]
    squeeze x3 -> x0, local copies, waits for them, and re-layouts: 5.74 us -> none  [gather_pieces(): lax.dynamic_index_in_dim(weight, lax.rem(me + by, nx), 0, keepdims=False)]
    ppermute x9 -> x0, starting transfers between devices: 3.7 us -> none  [swap(): return lax.ppermute(x, axis, [(i, (i + by) % size) for i in range(size)])]
  transfers between devices with their start and end apart: 13 -> 2, of which waited for: 5 -> 1; matrix products, arithmetic and copies ran while one was open for 19% -> 5% of each run, Pallas kernels for 0% -> 0%
where the time goes in v2:
time: 120 us
  Pallas kernels  86.8 us (72%)
  other arithmetic  9.59 us (8%)
  starting transfers between devices  8.36 us (7%)
  matrix products  5.85 us (5%)
  local copies, waits for them, and re-layouts  4.99 us (4%)
  waiting for transfers between devices  3.65 us (3%)
    pallas_call x1, Pallas kernels, run_experts(): pl.pallas_call(functools.partial(exchange_kernel, sp, local, slab_rows, g...  86.8 us
    ppermute x1, starting transfers between devices, body(): tail = lax.ppermute(tail, 'sp', [(i, i + 1) for i in range(sp_count - 1)])  4.91 us
    all_to_all x1, waiting for transfers between devices, body(): lax.all_to_all(result.astype(BF16), tp, split_axis=0, concat_axis=1, tile...  3.65 us
    convert_element_type x1, other arithmetic, body(): result.astype(BF16)  3.52 us
    all_to_all x1, starting transfers between devices, body(): lax.all_to_all(result.astype(BF16), tp, split_axis=0, concat_axis=1, tile...  3.45 us
    dot_general x1, matrix products, body(): lax.dot_general(both, routed, (((0,), (0,)), ((), ())), preferred_element...  2.4 us
  transfers between devices with their start and end apart: 2, of which 1 were waited for; matrix products, arithmetic and copies ran while one was open for 5% of the time, Pallas kernels for 0%

profile of v2, /device:TPU:0, one launch (start us, length us, event | category | flops | bytes accessed | tf_op | source)
XLA Modules:
  0.0 119.5 jit_solution(10520862357190849640)
XLA Ops:
  0.0 0.0 copy-start
  0.0 0.0 copy-start.3
  0.0 0.0 copy-start.4
  0.0 0.8 fusion.88
  0.8 0.1 slice.326
  0.9 0.7 slice.324
  1.6 0.7 slice.325
  2.3 0.1 pad.14.clone
  2.4 0.1 maximum_maximum_fusion
  2.5 4.9 %collective-permute-start = (bf16[90,128]{1,0:T(8,128)(2,1)S(1)}, bf16[90,128]{1,0:T(8,128)(2,1)S(1)}, u32[]{:S(2)}, u32[]{:S(2)}) collective-permute-start(bf16[90,128]{1,0:T(8,128)(2,1)S(1)} %maximum_maximum_fusion), channel_id=1, source_target_pairs={{0,4},{4,8},{8,12},{12,16},{16,20},{20,24},{24,28},{1,5},{5,9},{9,... | collective-permute-start | bytes 69128 | tf_op jit(solution)/shard_map/ppermute | solution.py:208
  7.4 0.8 slice_bitcast_fusion.1
  8.2 0.1 fusion.79
  8.3 1.0 slice_bitcast_fusion.32
  9.3 0.8 bitcast_multiply_fusion.1
  10.1 0.1 compare_and_fusion
  10.2 0.0 copy-start.8
  10.2 0.5 broadcast_and_fusion
  10.7 0.3 tile.11
  11.0 0.9 subtract_convert_fusion
  11.9 1.0 slice_bitcast_fusion.31
  12.9 0.0 collective-permute-done
  12.9 0.1 slice_reduce_fusion
  13.0 0.1 pad_maximum_fusion
  13.1 0.1 slice_compare_fusion.28
  13.2 0.1 slice_compare_fusion.29
  13.3 0.0 copy-done.3
  13.3 0.0 copy-done.4
  13.3 0.1 divide_multiply_fusion
  13.4 0.0 copy-done.8
  13.4 3.5 %fusion.15 = bf16[512,128]{1,0:T(8,128)(2,1)} fusion(f32[542,128]{1,0:T(8,128)S(1)} %divide_multiply_fusion, f32[128]{0:T(128)S(1)} %get-tuple-element.44, f32[128]{0:T(128)S(1)} %get-tuple-element.45, f32[128]{0:T(128)S(1)} %get-tuple-element.16, f32[128]{0:T(128)S(1)} %get-tuple-element.17, f32[128]{0:T(128)S(1)} %get-tuple-element.18, ...), kind=kLoop, calls=%fused_computation.29 | loop fusion | flops 6160384 | bytes 8289792 | tf_op jit(solution)/shard_map/convert_element_type | solution.py:219
  17.0 0.0 copy-start.6
  17.0 0.0 copy-start.7
  17.0 3.5 %all-to-all-start = ((bf16[4,128,128]{2,1,0:T(8,128)(2,1)}), bf16[4,128,128]{2,1,0:T(8,128)(2,1)S(1)}, u32[]{:S(2)}, u32[]{:S(2)}) async-start(bf16[4,128,128]{2,1,0:T(8,128)(2,1)} %bitcast.31), calls=%async_computation | async-start | bytes 262144 | tf_op jit(solution)/shard_map/all_to_all | solution.py:219
  20.4 0.9 fusion.8
  21.3 3.6 %all-to-all-done = bf16[4,128,128]{2,1,0:T(8,128)(2,1)S(1)} async-done(((bf16[4,128,128]{2,1,0:T(8,128)(2,1)}), bf16[4,128,128]{2,1,0:T(8,128)(2,1)S(1)}, u32[]{:S(2)}, u32[]{:S(2)}) %all-to-all-start) | async-done | bytes 131104 | tf_op jit(solution)/shard_map/all_to_all | solution.py:219
  25.0 0.1 copy.17
  25.1 0.1 convert_reduce_fusion
  25.3 0.0 copy-done.6
  25.3 0.0 copy-done.7
  25.3 0.0 copy-start.5
  25.3 0.2 multiply_convert_fusion.1
  25.5 0.0 copy-done
  25.5 1.6 %multiply_reduce_fusion = (f32[128]{0:T(128)S(1)}, f32[128,2048]{1,0:T(8,128)S(1)}) fusion(bf16[128,512]{0,1:T(8,128)(2,1)S(1)} %multiply_convert_fusion.1, bf16[512,2048]{1,0:T(8,128)(2,1)S(1)} %copy-done, bf16[128,2048]{1,0:T(8,128)(2,1)} %param.16), kind=kOutput, calls=%fused_computation.8 | convolution fusion | flops 270008192 | bytes 3801600 | tf_op jit(solution)/shard_map/dot_general | solution.py:225
  27.1 0.0 copy-done.5
  27.2 0.2 multiply_convert_fusion
  27.4 1.7 %convolution_convert_fusion = bf16[768,1024]{1,0:T(8,128)(2,1)} fusion(bf16[128,1024]{1,0:T(8,128)(2,1)S(1)} %get-tuple-element.12, bf16[128,1024]{1,0:T(8,128)(2,1)S(1)} %get-tuple-element.11, pred[96,8,2,128]{3,2,1,0:T(4,128)(4,1)S(1)} %bitcast.114), kind=kOutput, calls=%fused_computation.3 | convolution fusion | flops 404488192 | bytes 2293760 | tf_op jit(solution)/shard_map/dot_general | solution.py:252
  29.1 0.0 copy-start.1
  29.1 0.0 copy-start.2
  29.1 86.8 %shard_map.154 = bf16[16,48,1024]{2,1,0:T(8,128)(2,1)} custom-call(bf16[16,48,1024]{2,1,0:T(8,128)(2,1)} %bitcast.115, bf16[2,2048,256]{2,1,0:T(8,128)(2,1)} %gate_ref.1, bf16[2,2048,256]{2,1,0:T(8,128)(2,1)} %up_ref.1, bf16[2,256,2048]{2,1,0:T(8,128)(2,1)} %down_ref.1), custom_call_target="tpu_custom_call" | custom-call | tf_op jit(solution)/shard_map/pallas_call | solution.py:169
  115.9 0.0 copy-done.1
  115.9 0.0 copy-done.2
  115.9 2.4 %fusion.3 = f32[512,1024]{1,0:T(8,128)S(1)} fusion(bf16[768,1024]{1,0:T(8,128)(2,1)} %bitcast.116, bf16[768,256]{1,0:T(8,128)(2,1)S(1)} %copy-done.1, bf16[768,256]{1,0:T(8,128)(2,1)S(1)} %copy-done.2), kind=kOutput, calls=%fused_computation.10 | convolution fusion | flops 806879232 | bytes 4456448 | tf_op jit(solution)/shard_map/dot_general | solution.py:260
  118.3 0.1 slice_add_fusion
  118.5 0.1 fusion.89
  118.6 0.9 fusion.2
  (10 shorter events, 0.1 us)
Async XLA Ops:
  0.0 25.5 %copy-start = (bf16[512,2048]{1,0:T(8,128)(2,1)S(1)}, bf16[512,2048]{1,0:T(8,128)(2,1)}, u32[]{:S(2)}) copy-start(bf16[512,2048]{1,0:T(8,128)(2,1)} %param.24) | copy-start | bytes 6291460
  0.0 13.3 %copy-start.3 = (bf16[512,128]{1,0:T(8,128)(2,1)S(1)}, bf16[512,128]{1,0:T(8,128)(2,1)}, u32[]{:S(2)}) copy-start(bf16[512,128]{1,0:T(8,128)(2,1)} %param.17) | copy-start | bytes 393220
  0.0 13.3 %copy-start.4 = (bf16[512,128]{1,0:T(8,128)(2,1)S(1)}, bf16[512,128]{1,0:T(8,128)(2,1)}, u32[]{:S(2)}) copy-start(bf16[512,128]{1,0:T(8,128)(2,1)} %param.18) | copy-start | bytes 393220
  2.5 10.4 %collective-permute-start = (bf16[90,128]{1,0:T(8,128)(2,1)S(1)}, bf16[90,128]{1,0:T(8,128)(2,1)S(1)}, u32[]{:S(2)}, u32[]{:S(2)}) collective-permute-start(bf16[90,128]{1,0:T(8,128)(2,1)S(1)} %maximum_maximum_fusion), channel_id=1, source_target_pairs={{0,4},{4,8},{8,12},{12,16},{16,20},{20,24},{24,28},{1,5},{5,9},{9,... | collective-permute-start | bytes 69128 | tf_op jit(solution)/shard_map/ppermute | solution.py:208
  10.2 3.2 %copy-start.8 = (f32[128]{0:T(128)S(1)}, f32[128]{0:T(128)}, u32[]{:S(2)}) copy-start(f32[128]{0:T(128)} %param.21) | copy-start | bytes 1540
  17.0 8.3 %copy-start.6 = (f32[512]{0:T(512)S(1)}, f32[512]{0:T(512)}, u32[]{:S(2)}) copy-start(f32[512]{0:T(512)} %param.23) | copy-start | bytes 6148
  17.0 8.3 %copy-start.7 = (f32[512]{0:T(512)S(1)}, f32[512]{0:T(512)}, u32[]{:S(2)}) copy-start(f32[512]{0:T(512)} %param.22) | copy-start | bytes 6148
  17.0 8.0 %all-to-all-start = ((bf16[4,128,128]{2,1,0:T(8,128)(2,1)}), bf16[4,128,128]{2,1,0:T(8,128)(2,1)S(1)}, u32[]{:S(2)}, u32[]{:S(2)}) async-start(bf16[4,128,128]{2,1,0:T(8,128)(2,1)} %bitcast.31), calls=%async_computation | async-start | bytes 262144 | tf_op jit(solution)/shard_map/all_to_all | solution.py:219
  25.3 1.9 %copy-start.5 = (f32[2048]{0:T(1024)S(1)}, f32[2048]{0:T(1024)}, u32[]{:S(2)}) copy-start(f32[2048]{0:T(1024)} %param.25) | copy-start | bytes 24580
  29.1 86.8 %copy-start.1 = (bf16[768,256]{1,0:T(8,128)(2,1)S(1)}, bf16[768,256]{1,0:T(8,128)(2,1)}, u32[]{:S(2)}) copy-start(bf16[768,256]{1,0:T(8,128)(2,1)} %subtract_convert_fusion) | copy-start | bytes 1179652
  29.1 86.8 %copy-start.2 = (bf16[768,256]{1,0:T(8,128)(2,1)S(1)}, bf16[768,256]{1,0:T(8,128)(2,1)}, u32[]{:S(2)}) copy-start(bf16[768,256]{1,0:T(8,128)(2,1)} %fusion.8) | copy-start | bytes 1179652

commit v3 on v2

--- a/solution.py
+++ b/solution.py
@@ -192,32 +192,145 @@
     )(outgoing, expert_gate, expert_up, expert_down)
 
 
+def front_kernel(
+    sp, tp, capacity, halo,
+    value_ref, gate_ref, docs_ref, taps_ref, bias_ref, ids_ref, prob_ref, logits_ref,
+    cv_ref, picks_ref, spots_ref,
+    tails, acts, docs, conved, halo_sems, cv_sems,
+):
+    s, t = lax.axis_index("sp"), lax.axis_index("tp")
+    following, previous = (lax.rem(s + 1, sp), t), (lax.rem(s + sp - 1, sp), t)
+    barrier = pltpu.get_barrier_semaphore()
+    peers = [(s, flipped(t, d)) for d in range(1, tp)]
+    for where in [following, previous] + peers:
+        pl.semaphore_signal(barrier, inc=1, device_id=where, device_id_type=MESH)
+    block, chans = value_ref.shape
+    own_rows = block // tp
+    taps = taps_ref.shape[0]
+    value, gate = value_ref[...].astype(F32), gate_ref[...].astype(F32)
+    acts[halo:] = value * jax.nn.sigmoid(gate)
+    docs[halo:] = docs_ref[...].astype(F32)
+    pl.semaphore_wait(barrier, 2 + len(peers))
+    tail_copies = []
+    for k, ref in enumerate((value_ref, gate_ref, docs_ref)):
+        copy = pltpu.make_async_remote_copy(
+            src_ref=ref.at[pl.ds(block - halo, halo)], dst_ref=tails.at[k],
+            send_sem=halo_sems.at[0, k], recv_sem=halo_sems.at[1, k], device_id=following, device_id_type=MESH,
+        )
+        copy.start()
+        tail_copies.append(copy)
+
+    def convolve(q):
+        at = halo + q * own_rows
+        own_doc = docs[at : at + own_rows]
+        result = jnp.broadcast_to(bias_ref[...], (own_rows, chans))
+        for j in range(taps):
+            same = docs[at - j : at - j + own_rows] == own_doc
+            result = result + jnp.where(same, acts[at - j : at - j + own_rows], 0.0) * taps_ref[j : j + 1]
+        conved[q] = result.astype(BF16)
+
+    for q in range(1, tp):
+        convolve(q)
+    for copy in tail_copies:
+        copy.wait_recv()
+    tail_value, tail_gate = tails[0].astype(F32), tails[1].astype(F32)
+    acts[:halo] = tail_value * jax.nn.sigmoid(tail_gate)
+    docs[:halo] = jnp.where(s > 0, tails[2].astype(F32), -1.0)
+    convolve(0)
+    copies = []
+    for d in range(1, tp):
+        copy = pltpu.make_async_remote_copy(
+            src_ref=conved.at[flipped(t, d)], dst_ref=cv_ref.at[t],
+            send_sem=cv_sems.at[0, d], recv_sem=cv_sems.at[1, d],
+            device_id=(s, flipped(t, d)), device_id_type=MESH,
+        )
+        copy.start()
+        copies.append(copy)
+    cv_ref[t] = conved[t]
+
+    rows = 2 * capacity
+    experts = picks_ref.shape[0] // rows
+    top_count, tokens = ids_ref.shape
+    number = lax.broadcasted_iota(jnp.int32, (experts, tokens), 0)
+    gap = logits_ref[0:1] - logits_ref[1:2]
+    weights = [prob_ref[...] * jax.nn.sigmoid(gap), prob_ref[...] * jax.nn.sigmoid(-gap)]
+    named, weighted = 0.0, 0.0
+    for k in range(top_count):
+        name = jnp.where(number == ids_ref[k : k + 1], 1.0, 0.0)
+        named, weighted = named + name, weighted + name * weights[k]
+    earlier = lax.broadcasted_iota(jnp.int32, (tokens, tokens), 0)
+    later = lax.broadcasted_iota(jnp.int32, (tokens, tokens), 1)
+    before = jnp.where(earlier < later, 1.0, 0.0).astype(BF16)
+    ranks = jnp.dot(named.astype(BF16), before, preferred_element_type=F32)
+    ranks = jnp.where(named > 0.5, ranks, -1.0)
+    place = lax.broadcasted_iota(jnp.int32, (capacity, tokens), 0).astype(F32)
+    zeros = jnp.zeros((capacity, tokens), F32)
+
+    def both_halves(x):
+        return jnp.concatenate(
+            [jnp.concatenate([x, zeros], axis=1), jnp.concatenate([zeros, x], axis=1)], axis=0
+        ).astype(BF16)
+
+    for e in range(experts):
+        pick = jnp.where(place == ranks[e : e + 1], 1.0, 0.0)
+        spot = pick * weighted[e : e + 1]
+        high = spot.astype(BF16).astype(F32)
+        picks_ref[e * rows : (e + 1) * rows] = both_halves(pick)
+        spots_ref[e * rows : (e + 1) * rows, : 2 * tokens] = both_halves(high)
+        spots_ref[e * rows : (e + 1) * rows, 2 * tokens :] = both_halves(spot - high)
+    for copy in copies:
+        copy.wait()
+    for copy in tail_copies:
+        copy.wait_send()
+
+
+def front(conv_value, conv_gate, doc_ids, conv_taps, conv_bias, expert_ids, group_prob, route_logits, capacity, experts):
+    sp, tp = lax.axis_size("sp"), lax.axis_size("tp")
+    block, chans = conv_value.shape
+    halo = (conv_taps.shape[0] - 1 + 15) // 16 * 16
+    tokens = expert_ids.shape[0]
+    rows = experts * 2 * capacity
+    docs = jnp.broadcast_to(doc_ids.astype(BF16)[:, None], (block, chans))
+    pieces = (tp, block // tp, chans)
+    vmem = pl.BlockSpec(memory_space=pltpu.VMEM)
+    return pl.pallas_call(
+        functools.partial(front_kernel, sp, tp, capacity, halo),
+        out_shape=(
+            jax.ShapeDtypeStruct(pieces, BF16),
+            jax.ShapeDtypeStruct((rows, 2 * tokens), BF16),
+            jax.ShapeDtypeStruct((rows, 4 * tokens), BF16),
+        ),
+        in_specs=[vmem] * 8,
+        out_specs=(vmem,) * 3,
+        scratch_shapes=[
+            pltpu.VMEM((3, halo, chans), BF16),
+            pltpu.VMEM((halo + block, chans), F32),
+            pltpu.VMEM((halo + block, chans), F32),
+            pltpu.VMEM(pieces, BF16),
+            pltpu.SemaphoreType.DMA((2, 3)),
+            pltpu.SemaphoreType.DMA((2, tp)),
+        ],
+        compiler_params=pltpu.CompilerParams(collective_id=1, has_side_effects=True),
+    )(
+        conv_value, conv_gate, docs, conv_taps, conv_bias[None, :],
+        expert_ids.T, group_prob[None, :], route_logits.T,
+    )
+
+
 def body(
     stream, conv_value, conv_gate, doc_ids, conv_taps, conv_bias, chan_gain, chan_shift, out_weight,
     rms_gain, expert_ids, group_prob, route_logits, expert_gate, expert_up, expert_down,
 ):
-    reach = conv_taps.shape[0] - 1
-    tp = "tp"
     own_rows, width = stream.shape
-    sp_count = lax.axis_size("sp")
-    block, chans = conv_value.shape
-    docs_row = doc_ids.astype(BF16)
-    tail = jnp.concatenate(
-        [conv_value[-reach:], conv_gate[-reach:], jnp.broadcast_to(docs_row[-reach:, None], (reach, chans))], axis=0
+    experts_all = lax.axis_size("sp") * expert_gate.shape[0]
+    top_count = expert_ids.shape[1]
+    capacity = max(2, 3 * own_rows * top_count // (2 * experts_all))
+    capacity = (capacity + 7) // 8 * 8
+    conved, picks, spots = front(
+        conv_value, conv_gate, doc_ids, conv_taps, conv_bias, expert_ids, group_prob, route_logits,
+        capacity, experts_all,
     )
-    tail = lax.ppermute(tail, "sp", [(i, i + 1) for i in range(sp_count - 1)])
-
-    values = jnp.concatenate([tail[:reach], conv_value], axis=0).astype(F32)
-    gates = jnp.concatenate([tail[reach : 2 * reach], conv_gate], axis=0).astype(F32)
-    docs = jnp.concatenate([tail[2 * reach :, 0], docs_row], axis=0)
-    acts = values * jax.nn.sigmoid(gates)
-    result = jnp.broadcast_to(conv_bias[None, :], (block, chans))
-    for offset in range(reach + 1):
-        begin = reach - offset
-        same = (docs[begin : begin + block] == docs_row)[:, None]
-        result = result + jnp.where(same, acts[begin : begin + block], 0.0) * conv_taps[offset][None, :]
-    conved = lax.all_to_all(result.astype(BF16), tp, split_axis=0, concat_axis=1, tiled=True)
-
+    conved = jnp.swapaxes(conved, 0, 1).reshape(own_rows, -1)
     floats = conved.astype(F32)
     mean = jnp.mean(floats, axis=1, keepdims=True)
     spread = jnp.mean(floats * floats, axis=1, keepdims=True) - mean * mean
@@ -228,36 +341,11 @@
     mean_square = jnp.mean(resid_float * resid_float, axis=-1, keepdims=True)
     normed = (resid_float * lax.rsqrt(mean_square + eps) * rms_gain).astype(BF16)
 
-    local_experts = expert_gate.shape[0]
-    experts_all = sp_count * local_experts
-    top_count = expert_ids.shape[1]
-    capacity = max(2, 3 * own_rows * top_count // (2 * experts_all))
-    capacity = (capacity + 7) // 8 * 8
-    gap = route_logits[:, 0] - route_logits[:, 1]
-    weights = [group_prob * jax.nn.sigmoid(gap), group_prob * jax.nn.sigmoid(-gap)]
-    names = [
-        (jnp.arange(experts_all, dtype=jnp.int32)[:, None] == expert_ids[:, k][None, :]).astype(F32)
-        for k in range(top_count)
-    ]
-    named = sum(names)
-    weighted = sum(n * w[None, :] for n, w in zip(names, weights))
-    order = jnp.arange(own_rows, dtype=jnp.int32)
-    before = (order[:, None] < order[None, :]).astype(BF16)
-    ranks = jnp.dot(named.astype(BF16), before, preferred_element_type=F32)
-    slots = jnp.arange(capacity, dtype=jnp.int32).astype(F32)
-    picks = (ranks[:, None, :] == slots[None, :, None]) & (named[:, None, :] > 0)
-    side = jnp.eye(2, dtype=jnp.bool_)[None, :, None, :, None]
-    picks = (picks[:, None, :, None, :] & side).reshape(experts_all * 2 * capacity, 2 * own_rows)
     halves = jnp.concatenate([normed[:, : width // 2], normed[:, width // 2 :]], axis=0)
-    outgoing = jnp.dot(picks.astype(BF16), halves, preferred_element_type=F32).astype(BF16)
+    outgoing = jnp.dot(picks, halves, preferred_element_type=F32).astype(BF16)
     outgoing = outgoing.reshape(experts_all, 2 * capacity, width // 2)
     routed = run_experts(outgoing, expert_gate, expert_up, expert_down).reshape(-1, width // 2)
-    spread_weights = jnp.tile(jnp.repeat(weighted, 2 * capacity, axis=0), (1, 2))
-    spots = jnp.where(picks, spread_weights, 0.0)
-    high = spots.astype(BF16)
-    low = (spots - high.astype(F32)).astype(BF16)
-    both = jnp.concatenate([high, low], axis=1)
-    mixed = lax.dot_general(both, routed, (((0,), (0,)), ((), ())), preferred_element_type=F32)
+    mixed = lax.dot_general(spots, routed, (((0,), (0,)), ((), ())), preferred_element_type=F32)
     mixed = mixed[: 2 * own_rows] + mixed[2 * own_rows :]
     mixed = jnp.concatenate([mixed[:own_rows], mixed[own_rows:]], axis=1)
     return (resid_float + mixed).astype(BF16)

time: 120 us -> 113 us (0.942); the launches traced: 120 us -> 111 us
  Pallas kernels: 86.8 us -> 99.5 us
  starting transfers between devices: 8.36 us -> 0 us
  other arithmetic: 9.59 us -> 4.95 us
  waiting for transfers between devices: 3.65 us -> 0 us
  local copies, waits for them, and re-layouts: 4.99 us -> 1.85 us
    pallas_call x0 -> x1, Pallas kernels: none -> 14.3 us  [front(): pl.pallas_call(functools.partial(front_kernel, sp, tp, capacity, halo), o...]
    ppermute x1 -> x0, starting transfers between devices: 4.91 us -> none  [body(): tail = lax.ppermute(tail, 'sp', [(i, i + 1) for i in range(sp_count - 1)])]
    convert_element_type x4 -> x1, other arithmetic: 5.33 us -> 0.83 us  [front(): docs = jnp.broadcast_to(doc_ids.astype(BF16)[:, None], (block, chans))]
    all_to_all x1 -> x0, waiting for transfers between devices: 3.65 us -> none  [body(): lax.all_to_all(result.astype(BF16), tp, split_axis=0, concat_axis=1, tile...]
    all_to_all x1 -> x0, starting transfers between devices: 3.45 us -> none  [body(): lax.all_to_all(result.astype(BF16), tp, split_axis=0, concat_axis=1, tile...]
    mul x2 -> x0, local copies, waits for them, and re-layouts: 1.96 us -> none  [body(): jnp.where(same, acts[begin:begin + block], 0.0) * conv_taps[offset][None, :]]
    slice x5 -> x0, local copies, waits for them, and re-layouts: 1.6 us -> none  [the longest x1 0.7 us: body(): conv_gate[-reach:]]
    pallas_call x1, Pallas kernels: 86.8 us -> 85.2 us  [run_experts(): pl.pallas_call(functools.partial(exchange_kernel, sp, local, slab_rows, g...]
  transfers between devices with their start and end apart: 2 -> 0, of which waited for: 1 -> 0; matrix products, arithmetic and copies ran while one was open for 5% -> 0% of each run, Pallas kernels for 0% -> 0%
where the time goes in v3:
time: 113 us; the launch traced here: 111 us
  Pallas kernels  99.5 us (88%)
  other arithmetic  4.95 us (4%)
  matrix products  4.7 us (4%)
  local copies, waits for them, and re-layouts  1.85 us (2%)
    pallas_call x1, Pallas kernels, run_experts(): pl.pallas_call(functools.partial(exchange_kernel, sp, local, slab_rows, g...  85.2 us
    pallas_call x1, Pallas kernels, front(): pl.pallas_call(functools.partial(front_kernel, sp, tp, capacity, halo), o...  14.3 us
    dot_general x1, matrix products, body(): lax.dot_general(spots, routed, (((0,), (0,)), ((), ())), preferred_elemen...  2.4 us

profile of v3, /device:TPU:0, one launch (start us, length us, event | category | flops | bytes accessed | tf_op | source)
XLA Modules:
  0.0 111.1 jit_solution(16424803663517001766)
XLA Ops:
  0.0 0.0 copy-start
  0.0 0.0 copy-start.1
  0.0 0.8 convert_element_type.39
  0.8 0.8 broadcast_in_dim.6.docs_ref
  1.6 14.3 %shard_map.154 = (bf16[4,128,128]{2,1,0:T(8,128)(2,1)}, bf16[768,256]{1,0:T(8,128)(2,1)}, bf16[768,512]{1,0:T(8,128)(2,1)}) custom-call(bf16[512,128]{1,0:T(8,128)(2,1)} %value_ref.1, bf16[512,128]{1,0:T(8,128)(2,1)} %gate_ref.2, bf16[512,128]{1,0:T(8,128)(2,1)} %broadcast_in_dim.6.docs_ref, f32[31,128]{1,0:T(8,128)} %taps_ref.1, f32[1,128]{1,0:T(1,128)} %bitcast.27, ...), custom_call_target="tpu_custom_call" | custom-call | tf_op jit(solution)/shard_map/pallas_call | solution.py:296
  15.9 1.0 convert_reduce_fusion
  17.0 0.9 convert_bitcast_fusion
  17.9 0.1 copy.17
  18.0 0.0 copy-start.3
  18.0 0.9 multiply_convert_fusion.1
  19.0 0.0 copy-done
  19.0 0.0 copy-done.1
  19.0 0.6 multiply_reduce_fusion
  19.5 0.0 copy-start.2
  19.6 0.0 copy-done.3
  19.6 0.2 multiply_convert_fusion
  19.8 0.8 copy-done.2
  20.5 1.7 %convolution_convert_fusion = bf16[768,1024]{1,0:T(8,128)(2,1)} fusion(bf16[768,256]{1,0:T(8,128)(2,1)S(1)} %copy-done.2, bf16[128,1024]{1,0:T(8,128)(2,1)S(1)} %get-tuple-element.16, bf16[128,1024]{1,0:T(8,128)(2,1)S(1)} %get-tuple-element.15), kind=kOutput, calls=%fused_computation.3 | convolution fusion | flops 404488192 | bytes 2490368 | tf_op jit(solution)/shard_map/dot_general | solution.py:345
  22.3 0.0 copy-start.4
  22.3 85.2 %shard_map.155 = bf16[16,48,1024]{2,1,0:T(8,128)(2,1)} custom-call(bf16[16,48,1024]{2,1,0:T(8,128)(2,1)} %bitcast.23, bf16[2,2048,256]{2,1,0:T(8,128)(2,1)} %gate_ref.3, bf16[2,2048,256]{2,1,0:T(8,128)(2,1)} %up_ref.1, bf16[2,256,2048]{2,1,0:T(8,128)(2,1)} %down_ref.1), custom_call_target="tpu_custom_call" | custom-call | tf_op jit(solution)/shard_map/pallas_call | solution.py:169
  107.5 0.0 copy-done.4
  107.5 2.4 %fusion.13 = f32[512,1024]{1,0:T(8,128)S(1)} fusion(bf16[768,512]{1,0:T(8,128)(2,1)S(1)} %copy-done.4, bf16[768,1024]{1,0:T(8,128)(2,1)} %bitcast.24), kind=kOutput, calls=%fused_computation.27 | convolution fusion | flops 805306368 | bytes 4456448 | tf_op jit(solution)/shard_map/dot_general | solution.py:348
  109.9 0.1 slice_add_fusion
  110.0 0.1 fusion.11
  110.2 0.9 fusion.2
  (3 shorter events, 0.1 us)
Async XLA Ops:
  0.0 19.0 %copy-start = (bf16[512,2048]{1,0:T(8,128)(2,1)S(1)}, bf16[512,2048]{1,0:T(8,128)(2,1)}, u32[]{:S(2)}) copy-start(bf16[512,2048]{1,0:T(8,128)(2,1)} %param.24) | copy-start | bytes 6291460
  0.0 19.0 %copy-start.1 = (bf16[128,2048]{1,0:T(8,128)(2,1)S(1)}, bf16[128,2048]{1,0:T(8,128)(2,1)}, u32[]{:S(2)}) copy-start(bf16[128,2048]{1,0:T(8,128)(2,1)} %param.16) | copy-start | bytes 1572868
  18.0 1.5 %copy-start.3 = (f32[2048]{0:T(1024)S(1)}, f32[2048]{0:T(1024)}, u32[]{:S(2)}) copy-start(f32[2048]{0:T(1024)} %param.25) | copy-start | bytes 24580
  19.5 1.0 copy-start.2
  22.3 85.2 %copy-start.4 = (bf16[768,512]{1,0:T(8,128)(2,1)S(1)}, bf16[768,512]{1,0:T(8,128)(2,1)}, u32[]{:S(2)}) copy-start(bf16[768,512]{1,0:T(8,128)(2,1)} %get-tuple-element.9) | copy-start | bytes 2359300
